TPU v7x, 256 devices: a whole 4x4x8 slice. The times are simulated.
256 devices in a mesh: sp: 32 (over z, x), tp: 8 (over y, core).
Axes of the slice: x: 4, y: 4, z: 8, core: 2. Of those that a mesh axis runs over, the one named last changes fastest.
Arguments:
- tokens: bfloat16 [16384, 2048], P(('sp', 'tp')), may hold values from -6 to 6
- norm_gain: float32 [2048], replicated, may hold values from 0.1 to 1.9
- w_query: bfloat16 [2048, 1024], P(None, 'tp'), may hold values from -16 to 16
- w_key: bfloat16 [2048, 1024], P(None, 'tp'), may hold values from -16 to 16
- w_value: bfloat16 [2048, 1024], P(None, 'tp'), may hold values from -0.125 to 0.125
- conv_in: bfloat16 [2048, 2048], P(None, 'tp'), may hold values from -0.125 to 0.125
- conv_gate: bfloat16 [2048, 2048], P(None, 'tp'), may hold values from -0.125 to 0.125
- conv_taps: float32 [31, 2048], P(None, 'tp'), may hold values from -3.7 to 3.7
- conv_gain: float32 [2048], P('tp'), may hold values from 0.1 to 1.9
- cum_gate: float32 [16, 16384], P('tp'), may hold values from -2050 to 0, as said below
- out_attn: bfloat16 [1024, 2048], P('tp'), may hold values from -0.75 to 0.75
- out_conv: bfloat16 [2048, 2048], P('tp'), may hold values from -0.125 to 0.125
Outputs:
- mixed: bfloat16 [16384, 2048], P(('sp', 'tp'))
- log_total: float32 [16, 16384], P('tp', 'sp')
Inputs may be any that keep to these rules, and one draw needn't show every extreme that they name: `cum_gate`: for each head the values never rise from one position to the next and are at most 0.
All inputs are finite; a program needn't handle non-finite values.
Results may differ from a plain program's by a relative error of at most 0.014.
Values may be sent and summed in bfloat16 or wider, within the bound.
No kernel may reach another device: no remote copies, remote signals or barrier semaphores. Data moves between devices by JAX's collectives and lax.ppermute only.
A program may use at most 128 MiB of HBM per device.

v0:
```python
import math

import jax
import jax.numpy as jnp
from jax import lax
from jax.experimental import pallas as pl
from jax.experimental.pallas import tpu as pltpu
from jax.sharding import Mesh, PartitionSpec as P


HEAD = 64
LOG2E = math.log2(math.e)
LN2 = math.log(2.0)
NEG = -1e30
F32 = jnp.float32
BF16 = jnp.bfloat16
VMEM = pltpu.MemorySpace.VMEM
SMEM = pltpu.MemorySpace.SMEM
PARAMS = pltpu.CompilerParams(vmem_limit_bytes=24 * 2**20)


def vspec():
    return pl.BlockSpec(memory_space=VMEM)


def sspec():
    return pl.BlockSpec(memory_space=SMEM)


def turn(array, axis, by):
    n = lax.axis_size(axis)
    return lax.ppermute(array, axis, [(i, (i + by) % n) for i in range(n)])


def kernel(body, outs, args, scratch=(), aliases=None, scalars=1, far=False):
    spec = pl.BlockSpec(memory_space=pltpu.MemorySpace.HBM) if far else vspec()
    return pl.pallas_call(
        body,
        out_shape=outs,
        in_specs=[sspec()] * scalars + [spec] * (len(args) - scalars),
        out_specs=jax.tree.map(lambda _: vspec(), outs),
        scratch_shapes=list(scratch),
        input_output_aliases=aliases or {},
        compiler_params=PARAMS,
    )(*args)


def shape(*dims, dtype=BF16):
    return jax.ShapeDtypeStruct(dims, dtype)


def after(x, other):
    return lax.optimization_barrier((x, other))[0]


WIDTHS = (128, 128, 128, 256, 256)


def load_body(*refs):
    weights, out, sems = refs[:5], refs[5], refs[6]
    copies, at = [], 0
    for k, (ref, width) in enumerate(zip(weights, WIDTHS)):
        copies.append(pltpu.make_async_copy(ref, out.at[:, at : at + width], sems.at[k]))
        at += width
    for copy in copies:
        copy.start()
    for copy in copies:
        copy.wait()


def project_body(
    place, n0, n1, n2, n3, p0, p1, p2, p3, weights, q_out, kv_out, gated_out, rim_out, xs
):
    y = place[0]
    c = place[1]
    for k, (own, other) in enumerate(((n0, p0), (n1, p1), (n2, p2), (n3, p3))):
        at = lax.rem(y + 4 - k, 4) * 128
        xs[pl.ds(pl.multiple_of(at + c * 64, 64), 64), :] = own[...]
        xs[pl.ds(pl.multiple_of(at + (1 - c) * 64, 64), 64), :] = other[...]
    x = xs[...]
    qk = jnp.dot(x, weights[:, :256], preferred_element_type=F32)
    q_out[...] = jnp.transpose(qk[:, :128] * (LOG2E * HEAD**-0.5)).astype(BF16)
    kv_out[:512, :] = qk[:, 128:].astype(BF16)
    v = jnp.transpose(jnp.dot(x, weights[:, 256:384], preferred_element_type=F32)).astype(BF16)
    for j in range(4):
        kv_out[512 + 128 * j : 640 + 128 * j, :] = v[:, 128 * j : 128 * j + 128]
    opened = jnp.dot(x, weights[:, 384:640], preferred_element_type=F32)
    gating = jnp.dot(x, weights[:, 640:], preferred_element_type=F32)
    gated = (opened * jax.nn.sigmoid(gating)).astype(BF16)
    gated_out[...] = gated
    rim_out[...] = gated[480:]


def norm_body(tokens_far, gain_far, out, tokens, gain, sems):
    copies = [
        pltpu.make_async_copy(tokens_far, tokens, sems.at[0]),
        pltpu.make_async_copy(gain_far, gain, sems.at[1]),
    ]
    for copy in copies:
        copy.start()
    for copy in copies:
        copy.wait()
    wide = tokens[...].astype(F32)
    factor = lax.rsqrt(jnp.mean(wide * wide, axis=1, keepdims=True) + 1e-06)
    out[...] = (wide * factor * gain[...]).astype(BF16)


def bias_body(place, cum, bias, own):
    z = place[2]
    x = place[3]
    base = cum[:, pl.ds(pl.multiple_of(z * 2048, 128), 128)][:, :1]
    for b in range(8):
        at = pl.multiple_of((4 * b + x) * 512, 512)
        rel = (base - cum[:, pl.ds(at, 512)]) * LOG2E
        hi = rel.astype(BF16).astype(F32)
        mid = (rel - hi).astype(BF16).astype(F32)
        low = rel - hi - mid
        rows = [part[h : h + 1] for h in range(2) for part in (hi, mid, low)]
        rows = jnp.concatenate(rows + [jnp.zeros((122, 512), F32)], axis=0)
        bias[b] = jnp.transpose(rows).astype(BF16)
    at = pl.multiple_of((4 * z + x) * 512, 512)
    own[...] = cum[:, pl.ds(at, 512)] - base


def conv_body(gated, rim, taps, convolved, square, shifted):
    whole = jnp.concatenate([rim[...], gated[...]], axis=0).astype(F32)
    shifted[0] = whole
    for s in range(1, 8):
        shifted[s, :536] = whole[s : s + 536]

    def block(i, carry):
        at = pl.multiple_of(i * 128, 128)
        total = jnp.zeros((128, 256), F32)
        for tap in range(31):
            a, s = divmod(tap + 2, 8)
            total = total + taps[tap : tap + 1, :] * shifted[s, pl.ds(at + 8 * a, 128), :]
        convolved[pl.ds(at, 128), :] = total
        both = total * total
        both = jnp.transpose(both[:, :128] + both[:, 128:])
        square[:, pl.ds(at, 128)] = jnp.sum(both, axis=0, keepdims=True)
        return carry

    lax.fori_loop(0, 4, block, 0)


def gate_body(place, convolved, s0, s1, s2, s3, gain, weights, mine, theirs, left):
    c = place[1]
    square = (s0[...] + s1[...] + s2[...] + s3[...]) / 2048.0
    column = jnp.transpose(jnp.broadcast_to(lax.rsqrt(square + 1e-06), (128, 512)))
    factor = jnp.concatenate([column, column], axis=1)
    v = convolved[...] * factor * gain[...]
    left[...] = (v / (1.0 + jnp.exp(-v))).astype(BF16)

    def block(y, carry):
        rows = left[pl.ds(pl.multiple_of(128 * y, 128), 128), :]
        part = jnp.dot(rows, weights[...], preferred_element_type=F32).astype(BF16)

        @pl.when(c == 0)
        def _():
            mine[y] = part[:64]
            theirs[y] = part[64:]

        @pl.when(c == 1)
        def _():
            mine[y] = part[64:]
            theirs[y] = part[:64]

        return carry

    lax.fori_loop(0, 4, block, 0)


def fold_body(place, mine, theirs, own, f1, f2, f3):
    y = place[0]
    for k, ref in enumerate((own, f1, f2, f3)):
        at = lax.rem(y + k, 4)
        total = mine[at].astype(F32) + theirs[at].astype(F32)
        ref[...] = total.astype(ref.dtype)


def part_body(place, own, h0, h1, h2, h3, w0, w1, w2a, w2b, w3, mine, theirs):
    c = place[1]
    left = jnp.concatenate([h0[...], h1[...], h2[...], h3[...]], axis=1)
    right = jnp.concatenate([w0[...], w1[...], w2a[...], w2b[...], w3[...]], axis=0)
    both = jnp.dot(left, right, preferred_element_type=F32)

    @pl.when(c == 0)
    def _():
        mine[...] = both[:64] + own[...]
        theirs[...] = both[64:].astype(BF16)

    @pl.when(c == 1)
    def _():
        mine[...] = both[64:] + own[...]
        theirs[...] = both[:64].astype(BF16)


def final_body(mine, theirs, f1, f2, f3, out):
    folded = f1[...].astype(F32) + f2[...].astype(F32) + f3[...].astype(F32)
    out[...] = (mine[...] + theirs[...].astype(F32) + folded).astype(BF16)


DEPTH = 4


def tiles_of(slots):
    return [(s, h, lo) for s in range(slots) for h in range(2) for lo in (0, 256)]


def scores_tile(tile, at, q, kv, bias, slot, s_buf, top, offset):
    _, h, lo = tile
    block = q[slot, h * HEAD : (h + 1) * HEAD, lo : lo + 256]
    zero = jnp.zeros((HEAD, 256), BF16)
    row = lax.broadcasted_iota(jnp.int32, (128, 256), 0)
    pick = jnp.where((row >= 3 * h) & (row < 3 * h + 3), 1.0, 0.0).astype(BF16)
    rhs = jnp.concatenate([block, zero, pick] if h == 0 else [zero, block, pick], axis=0)
    lhs = jnp.concatenate([kv[:512, :], bias[...]], axis=1)
    s = jnp.dot(lhs, rhs, preferred_element_type=F32)
    if offset is not None:
        kk = lax.broadcasted_iota(jnp.int32, (512, 256), 0)
        qq = lax.broadcasted_iota(jnp.int32, (512, 256), 1) + (lo + offset)
        s = jnp.where(kk <= qq, s, NEG)
    s_buf[at % DEPTH] = s
    top[at % DEPTH] = jnp.max(s, axis=0, keepdims=True)


def weights_tile(tile, at, slot, best, s_buf, top, p_buf, shrink):
    _, h, lo = tile
    old = best[slot, h, :, lo : lo + 256]
    new = jnp.maximum(old, top[at % DEPTH])
    p_buf[at % DEPTH] = jnp.exp2(s_buf[at % DEPTH] - new).astype(BF16)
    best[slot, h, :, lo : lo + 256] = new
    shrink[at % DEPTH] = jnp.exp2(old - new)


def values_tile(tile, at, kv, slot, acc, p_buf, shrink):
    _, h, lo = tile
    vT = jnp.concatenate(
        [kv[512 + 128 * j + h * HEAD : 512 + 128 * j + (h + 1) * HEAD, :] for j in range(4)],
        axis=1,
    )
    vT = jnp.concatenate([vT, jnp.ones((16, 512), BF16)], axis=0)
    pv = jnp.dot(vT, p_buf[at % DEPTH], preferred_element_type=F32)
    acc[slot, h, :, lo : lo + 256] = (
        acc[slot, h, :, lo : lo + 256] * shrink[at % DEPTH] + pv
    )


def run_items(
    slots, count, block_of, bias_of, slot_of, offset_of, q, kvs, bias, acc, best, s_buf, top, p_buf, shrink
):
    tiles = tiles_of(slots)
    n = len(tiles)
    p_buf[(n - 1) % DEPTH] = jnp.zeros(p_buf.shape[1:], BF16)
    shrink[(n - 1) % DEPTH] = jnp.ones(shrink.shape[1:], F32)

    def scores(t, i):
        offset = None if offset_of is None else offset_of(i)
        slot = slot_of(i) + tiles[t][0]
        kv = kvs.at[block_of(i)]
        scores_tile(tiles[t], t, q, kv, bias.at[bias_of(i)], slot, s_buf, top, offset)

    def values(t, i):
        slot = slot_of(i) + tiles[t][0]
        values_tile(tiles[t], t, kvs.at[block_of(i)], slot, acc, p_buf, shrink)

    scores(0, 0)

    def step(i, carry):
        before = jnp.maximum(i - 1, 0)
        behind = jnp.minimum(i + 1, count - 1)
        for t in range(n):
            if t < n - 1:
                scores(t + 1, i)
            else:
                scores(0, behind)
            weights_tile(tiles[t], t, slot_of(i) + tiles[t][0], best, s_buf, top, p_buf, shrink)
            if t > 0:
                values(t - 1, i)
            else:
                values(n - 1, before)
        return carry

    lax.fori_loop(0, count, step, 0)
    values(n - 1, count - 1)


STATE = (
    jax.ShapeDtypeStruct((4, 2, 80, 512), F32),
    jax.ShapeDtypeStruct((4, 2, 1, 512), F32),
)


def attend_scratch(blocks):
    return [
        pltpu.VMEM((blocks, 1024, 128), BF16),
        pltpu.VMEM((DEPTH, 512, 256), F32),
        pltpu.VMEM((DEPTH, 1, 256), F32),
        pltpu.VMEM((DEPTH, 512, 256), BF16),
        pltpu.VMEM((DEPTH, 1, 256), F32),
    ]


def first_body(place, q0, q1, q2, q3, kv, bias, acc, best, q, kvs, s_buf, top, p_buf, shrink):
    z = place[2]
    x = place[3]
    for k, ref in enumerate((q0, q1, q2, q3)):
        q[k] = ref[...]
    kvs[0] = kv[...]
    acc[...] = jnp.zeros(acc.shape, F32)
    best[...] = jnp.full(best.shape, NEG, F32)
    run_items(
        1,
        4 - x,
        lambda i: 0,
        lambda i: z,
        lambda i: jnp.where(i == 0, 0, x + i),
        lambda i: jnp.where(i == 0, 0, 512),
        q, kvs, bias, acc, best, s_buf, top, p_buf, shrink,
    )


def more_body(shifts, last, place, q, bias, *refs):
    n = len(shifts)
    m = n + last
    blocks = refs[:m]
    if last:
        outs = refs[m + 2 : m + 6]
        acc, best, kvs, s_buf, top, p_buf, shrink = refs[m + 6 :]
    else:
        acc, best, kvs, s_buf, top, p_buf, shrink = refs[m + 2 :]
    z = place[2]
    count = 0
    for shift in shifts:
        count = count + jnp.where(z >= shift % 8, 2, 0)

    def source(b):
        shift = jnp.int32(shifts[-1])
        for k in range(n - 1):
            shift = jnp.where(b == k, shifts[k], shift)
        return lax.rem(z - shift + 8, 8)

    @pl.when(count > 0)
    def _():
        if last:
            kvs[0] = blocks[0][...]
            kvs[1, :512] = blocks[1][...]
            kvs[1, 512:] = blocks[2][...]
            kvs[2] = blocks[3][...]
        else:
            for k, ref in enumerate(blocks):
                kvs[k] = ref[...]

        def block(i):
            return i // 2 if isinstance(i, int) else lax.shift_right_logical(i, 1)

        run_items(
            2,
            count,
            block,
            lambda i: source(block(i)),
            lambda i: 2 * (i % 2) if isinstance(i, int) else 2 * lax.bitwise_and(i, 1),
            None,
            q, kvs, bias, acc, best, s_buf, top, p_buf, shrink,
        )

    if last:
        for slot in range(4):
            stats = []
            for h in range(2):
                total = acc[slot, h, 64:65, :]
                total = jnp.where(total > 0.0, total, 1.0)
                outs[slot][h * HEAD : (h + 1) * HEAD, :] = (
                    acc[slot, h, :HEAD, :] / total
                ).astype(BF16)
                log_sum = best[slot, h] + jnp.log2(total)
                hi = log_sum.astype(BF16).astype(F32)
                mid = (log_sum - hi).astype(BF16).astype(F32)
                low = log_sum - hi - mid
                stats += [hi, mid, low]
            stats.append(jnp.zeros((10, 512), F32))
            outs[slot][128:144, :] = jnp.concatenate(stats, axis=0).astype(BF16)


def attend_first(place, qs, kv, bias):
    return kernel(
        first_body, STATE + (shape(4, 128, 512),), (place, *qs, kv, bias), attend_scratch(1)
    )


def attend_more(place, q, bias, kvs, shifts, state, last=False):
    def body(*refs):
        more_body(shifts, last, *refs)

    if last:
        first, (upper, lower), third = kvs
        kvs = (first, upper, lower, third)
    n = len(kvs)
    outs = (shape(144, 512),) * 4 if last else ()
    aliases = {3 + n: len(outs), 4 + n: len(outs) + 1}
    scratch = attend_scratch(len(shifts))
    return kernel(body, outs + STATE, (place, q, bias, *kvs, *state), scratch, aliases)


def merge_body(place, own, r1, r2, r3, cum, log_out, *refs):
    pieces, rows = refs[:4], refs[4]
    y = place[0]
    parts = (own, r1, r2, r3)
    for h in range(2):
        logs = []
        for part in parts:
            stats = part[128:144, :].astype(F32)
            logs.append(
                stats[3 * h : 3 * h + 1] + stats[3 * h + 1 : 3 * h + 2] + stats[3 * h + 2 : 3 * h + 3]
            )
        peak = jnp.maximum(jnp.maximum(logs[0], logs[1]), jnp.maximum(logs[2], logs[3]))
        ws = [jnp.exp2(v - peak) for v in logs]
        total = ws[0] + ws[1] + ws[2] + ws[3]
        o = jnp.zeros((HEAD, 512), F32)
        for part, w in zip(parts, ws):
            o = o + part[h * HEAD : (h + 1) * HEAD, :].astype(F32) * w
        rows[:, h * HEAD : (h + 1) * HEAD] = jnp.transpose(o / total)
        log_out[h : h + 1, :] = (peak + jnp.log2(total)) * LN2 + cum[h : h + 1, :]
    for k in range(4):
        at = pl.multiple_of(lax.rem(y + k, 4) * 128, 128)
        pieces[k][...] = rows[pl.ds(at, 128), :].astype(BF16)


def per_device(
    tokens,
    norm_gain,
    w_query,
    w_key,
    w_value,
    conv_in,
    conv_gate,
    conv_taps,
    conv_gain,
    cum_gate,
    out_attn,
    out_conv,
):
    z = lax.axis_index("z")
    x = lax.axis_index("x")
    y = lax.axis_index("y")
    c = lax.axis_index("c")
    place = jnp.stack([y, c, z, x]).astype(jnp.int32)

    n0 = kernel(
        norm_body,
        shape(64, 2048),
        (tokens, norm_gain[None, :]),
        [
            pltpu.VMEM((64, 2048), BF16),
            pltpu.VMEM((1, 2048), F32),
            pltpu.SemaphoreType.DMA((2,)),
        ],
        scalars=0,
        far=True,
    )
    own = [n0] + [turn(n0, "y", k) for k in (1, 2, 3)]
    partner = [turn(piece, "c", 1) for piece in own]

    weights = kernel(
        load_body,
        shape(2048, 896),
        (w_query, w_key, w_value, conv_in, conv_gate),
        [pltpu.SemaphoreType.DMA((5,))],
        scalars=0,
        far=True,
    )
    bias, cum_own = kernel(
        bias_body, (shape(8, 512, 128), shape(2, 512, dtype=F32)), (place, cum_gate)
    )

    qT, kv, gated, rim = kernel(
        project_body,
        (shape(128, 512), shape(1024, 128), shape(512, 256), shape(32, 256)),
        (place, *own, *partner, weights),
        [pltpu.VMEM((512, 2048), BF16)],
    )

    rim = lax.ppermute(rim, ("z", "x"), [(i, i + 1) for i in range(31)])
    a1 = turn(kv, "z", 1)
    b1 = turn(kv, "z", -1)
    qs = [qT] + [turn(qT, "x", k) for k in (1, 2, 3)]
    a2 = turn(a1, "z", 1)
    b2 = turn(b1, "z", -1)
    a3 = turn(a2, "z", 1)
    b3 = turn(b2, "z", -1)
    fa = turn(a3[:512], "z", 1)
    fb = turn(b3[512:], "z", -1)

    convolved, square = kernel(
        conv_body,
        (shape(512, 256, dtype=F32), shape(1, 512, dtype=F32)),
        (gated, rim, conv_taps),
        [pltpu.VMEM((8, 544, 256), F32)],
        scalars=0,
    )
    square = square + turn(square, "c", 1)
    squares = [square] + [turn(square, "y", k) for k in (1, 2, 3)]
    mine, theirs = kernel(
        gate_body,
        (shape(4, 64, 2048), shape(4, 64, 2048)),
        (place, convolved, *squares, conv_gain[None, :], out_conv),
        [pltpu.VMEM((512, 256), BF16)],
    )
    theirs = turn(theirs, "c", 1)
    folded = kernel(
        fold_body, (shape(64, 2048, dtype=F32),) + (shape(64, 2048),) * 3, (place, mine, theirs)
    )
    folded = [folded[0]] + [turn(folded[k], "y", k) for k in (1, 2, 3)]

    w0 = after(out_attn, kv)
    w1 = turn(w0, "y", 1)
    w3 = turn(w0, "y", 3)
    w2a = turn(w1[:64], "y", 1)
    w2b = turn(w3[64:], "y", 3)

    *state, q = attend_first(place, qs, kv, bias)
    state = attend_more(place, q, bias, (a1, b1), (1, -1), state)
    state = attend_more(place, q, bias, (a2, b2), (2, -2), state)
    outs = attend_more(place, q, bias, (a3, (fa, fb), b3), (3, 4, -3), state, True)
    others = [turn(outs[k], "x", -k) for k in (1, 2, 3)]
    log_total, *pieces = kernel(
        merge_body,
        (shape(2, 512, dtype=F32),) + (shape(128, 128),) * 4,
        (place, outs[0], *others, cum_own),
        [pltpu.VMEM((512, 128), F32)],
    )
    heads = [pieces[0]] + [turn(pieces[k], "y", k) for k in (1, 2, 3)]
    mine, theirs = kernel(
        part_body,
        (shape(64, 2048, dtype=F32), shape(64, 2048)),
        (place, folded[0], *heads, w0, w1, w2a, w2b, w3),
    )
    theirs = turn(theirs, "c", 1)
    mixed = kernel(final_body, shape(64, 2048), (mine, theirs, *folded[1:]), scalars=0)
    return (mixed, log_total)


def solution(mesh):
    grid = Mesh(mesh.devices.reshape(8, 4, 4, 2), ("z", "x", "y", "c"))
    sp = ("z", "x")
    tp = ("y", "c")
    in_specs = (
        P(sp + tp, None),
        P(),
        P(None, tp),
        P(None, tp),
        P(None, tp),
        P(None, tp),
        P(None, tp),
        P(None, tp),
        P(tp),
        P(tp, None),
        P(tp, None),
        P(tp, None),
    )
    out_specs = (P(sp + tp, None), P(tp, sp))

    return jax.shard_map(
        per_device, mesh=grid, in_specs=in_specs, out_specs=out_specs, check_vma=False
    )
```

profile of v0, /device:TPU:230, one launch (start us, length us, event | category | flops | bytes accessed | tf_op | source)
XLA Modules:
  0.0 138.2 jit_solution(5436476036740303072)
XLA Ops:
  4.1 2.9 %collective-permute-start.1 = (bf16[64,2048]{1,0:T(8,128)(2,1)S(1)}, bf16[64,2048]{1,0:T(8,128)(2,1)S(1)}, u32[]{:S(2)}, u32[]{:S(2)}) collective-permute-start(bf16[64,2048]{1,0:T(8,128)(2,1)S(1)} %shard_map.131.n0), channel_id=1, source_target_pairs={{0,4},{2,6},{4,0},{6,2},{1,5},{3,7},{5,1},{7,3},{8,12},{10,14},{12... | collective-permute-start | bytes 786440 | tf_op jit(solution)/shard_map/ppermute | solution.py:32
  8.4 3.5 %collective-permute-done.n1 = bf16[64,2048]{1,0:T(8,128)(2,1)S(1)} collective-permute-done((bf16[64,2048]{1,0:T(8,128)(2,1)S(1)}, bf16[64,2048]{1,0:T(8,128)(2,1)S(1)}, u32[]{:S(2)}, u32[]{:S(2)}) %collective-permute-start) | collective-permute-done | bytes 262176 | tf_op jit(solution)/shard_map/ppermute | solution.py:32
  11.9 6.8 %collective-permute-done.1.n2 = bf16[64,2048]{1,0:T(8,128)(2,1)S(1)} collective-permute-done((bf16[64,2048]{1,0:T(8,128)(2,1)S(1)}, bf16[64,2048]{1,0:T(8,128)(2,1)S(1)}, u32[]{:S(2)}, u32[]{:S(2)}) %collective-permute-start.1) | collective-permute-done | bytes 262176 | tf_op jit(solution)/shard_map/ppermute | solution.py:32
  25.4 3.0 %shard_map.133 = (bf16[128,512]{1,0:T(8,128)(2,1)S(1)}, bf16[1024,128]{1,0:T(8,128)(2,1)S(1)}, bf16[512,256]{1,0:T(8,128)(2,1)S(1)}, bf16[32,256]{1,0:T(8,128)(2,1)S(1)}) custom-call(s32[4]{0:T(128)S(1)} %pad_add_fusion.place.refs_0_, bf16[64,2048]{1,0:T(8,128)(2,1)S(1)} %shard_map.131.n0, bf16[64,2048]{1,0:T(8,128)(2,1)S(1)} %collective-permute-done.n1, ...), custom_call_target="tpu_custom_call" | custom-call | tf_op jit(solution)/shard_map/pallas_call | solution.py:37
  28.5 2.0 %collective-permute-start.20 = (bf16[1024,128]{1,0:T(8,128)(2,1)S(1)}, bf16[1024,128]{1,0:T(8,128)(2,1)S(1)}, u32[]{:S(2)}, u32[]{:S(2)}) collective-permute-start(bf16[1024,128]{1,0:T(8,128)(2,1)S(1)} %get-tuple-element.43.kv), channel_id=1, source_target_pairs={{0,224},{32,0},{64,32},{96,64},{128,96},{160,128},{192,160},{224,1... | collective-permute-start | bytes 786440 | tf_op jit(solution)/shard_map/ppermute | solution.py:32
  30.5 6.2 %collective-permute-done.16.refs_3_ = bf16[1024,128]{1,0:T(8,128)(2,1)S(1)} collective-permute-done((bf16[1024,128]{1,0:T(8,128)(2,1)S(1)}, bf16[1024,128]{1,0:T(8,128)(2,1)S(1)}, u32[]{:S(2)}, u32[]{:S(2)}) %collective-permute-start.16) | collective-permute-done | bytes 262176 | tf_op jit(solution)/shard_map/ppermute | solution.py:32
  40.0 4.3 %collective-permute-done.7.rim = bf16[32,256]{1,0:T(8,128)(2,1)S(1)} collective-permute-done((bf16[32,256]{1,0:T(8,128)(2,1)S(1)}, bf16[32,256]{1,0:T(8,128)(2,1)S(1)}, u32[]{:S(2)}, u32[]{:S(2)}) %collective-permute-start.7) | collective-permute-done | bytes 16416 | tf_op jit(solution)/shard_map/ppermute | solution.py:483
  44.4 2.2 %shard_map.134 = (f32[512,256]{1,0:T(8,128)S(1)}, f32[1,512]{1,0:T(1,128)S(1)}) custom-call(bf16[512,256]{1,0:T(8,128)(2,1)S(1)} %get-tuple-element.35.gated, bf16[32,256]{1,0:T(8,128)(2,1)S(1)} %collective-permute-done.7.rim, f32[31,256]{1,0:T(8,128)S(1)} %copy-done.9), custom_call_target="tpu_custom_call" | custom-call | tf_op jit(solution)/shard_map/pallas_call | solution.py:37
  47.8 2.6 %collective-permute-start.10 = (f32[1,512]{1,0:T(1,128)S(1)}, f32[1,512]{1,0:T(1,128)S(1)}, u32[]{:S(2)}, u32[]{:S(2)}) collective-permute-start(f32[1,512]{1,0:T(1,128)S(1)} %add.3.s0), channel_id=1, source_target_pairs={{0,4},{2,6},{4,0},{6,2},{1,5},{3,7},{5,1},{7,3},{8,12},{10,14},{12... | collective-permute-start | bytes 6152 | tf_op jit(solution)/shard_map/ppermute | solution.py:32
  54.0 2.6 %collective-permute-done.9.s1 = f32[1,512]{1,0:T(1,128)S(1)} collective-permute-done((f32[1,512]{1,0:T(1,128)S(1)}, f32[1,512]{1,0:T(1,128)S(1)}, u32[]{:S(2)}, u32[]{:S(2)}) %collective-permute-start.9) | collective-permute-done | bytes 2080 | tf_op jit(solution)/shard_map/ppermute | solution.py:32
  56.6 2.3 %shard_map.135 = (bf16[4,64,2048]{2,1,0:T(8,128)(2,1)S(1)}, bf16[4,64,2048]{2,1,0:T(8,128)(2,1)S(1)}) custom-call(s32[4]{0:T(128)S(1)} %pad_add_fusion.place.refs_0_, f32[512,256]{1,0:T(8,128)S(1)} %get-tuple-element.37.convolved, f32[1,512]{1,0:T(1,128)S(1)} %add.3.s0, f32[1,512]{1,0:T(1,128)S(1)} %collective-permute-done.9.s1, ...), custom_call_target="tpu_custom_call" | custom-call | tf_op jit(solution)/shard_map/pallas_call | solution.py:37
  58.9 3.3 %collective-permute-start.13 = (bf16[128,512]{1,0:T(8,128)(2,1)S(1)}, bf16[128,512]{1,0:T(8,128)(2,1)S(1)}, u32[]{:S(2)}, u32[]{:S(2)}) collective-permute-start(bf16[128,512]{1,0:T(8,128)(2,1)S(1)} %get-tuple-element.42.q0), channel_id=1, source_target_pairs={{0,8},{8,16},{16,24},{24,0},{1,9},{9,17},{17,25},{25,1},{2,10},{10... | collective-permute-start | bytes 393224 | tf_op jit(solution)/shard_map/ppermute | solution.py:32
  62.2 2.0 %collective-permute-start.22 = (bf16[1024,128]{1,0:T(8,128)(2,1)S(1)}, bf16[1024,128]{1,0:T(8,128)(2,1)S(1)}, u32[]{:S(2)}, u32[]{:S(2)}) collective-permute-start(bf16[1024,128]{1,0:T(8,128)(2,1)S(1)} %collective-permute-done.21.refs_4_), channel_id=1, source_target_pairs={{0,224},{32,0},{64,32},{96,64},{128,96},{160,128},{192,160},{224,1... | collective-permute-start | bytes 786440 | tf_op jit(solution)/shard_map/ppermute | solution.py:32
  67.5 3.1 %collective-permute-done.18.refs_3_ = bf16[1024,128]{1,0:T(8,128)(2,1)S(1)} collective-permute-done((bf16[1024,128]{1,0:T(8,128)(2,1)S(1)}, bf16[1024,128]{1,0:T(8,128)(2,1)S(1)}, u32[]{:S(2)}, u32[]{:S(2)}) %collective-permute-start.18) | collective-permute-done | bytes 262176 | tf_op jit(solution)/shard_map/ppermute | solution.py:32
  73.0 5.1 %collective-permute-done.14.q2 = bf16[128,512]{1,0:T(8,128)(2,1)S(1)} collective-permute-done((bf16[128,512]{1,0:T(8,128)(2,1)S(1)}, bf16[128,512]{1,0:T(8,128)(2,1)S(1)}, u32[]{:S(2)}, u32[]{:S(2)}) %collective-permute-start.14) | collective-permute-done | bytes 131104 | tf_op jit(solution)/shard_map/ppermute | solution.py:32
  83.6 6.2 %shard_map.139 = (f32[4,2,80,512]{3,2,1,0:T(8,128)S(1)}, f32[4,2,1,512]{3,2,1,0:T(1,128)S(1)}) custom-call(s32[4]{0:T(128)S(1)} %pad_add_fusion.place.refs_0_, bf16[4,128,512]{2,1,0:T(8,128)(2,1)S(1)} %get-tuple-element.45.refs_1_, bf16[8,512,128]{2,1,0:T(8,128)(2,1)S(1)} %get-tuple-element.44.bias.refs_2_, ...), custom_call_target="tpu_custom_call", output_to_operand_aliasing={{0}: (5, {}), {1}: (6, {})} | custom-call | tf_op jit(solution)/shard_map/pallas_call | solution.py:37
  89.8 6.4 %shard_map.140 = (f32[4,2,80,512]{3,2,1,0:T(8,128)S(1)}, f32[4,2,1,512]{3,2,1,0:T(1,128)S(1)}) custom-call(s32[4]{0:T(128)S(1)} %pad_add_fusion.place.refs_0_, bf16[4,128,512]{2,1,0:T(8,128)(2,1)S(1)} %get-tuple-element.45.refs_1_, bf16[8,512,128]{2,1,0:T(8,128)(2,1)S(1)} %get-tuple-element.44.bias.refs_2_, ...), custom_call_target="tpu_custom_call", output_to_operand_aliasing={{0}: (5, {}), {1}: (6, {})} | custom-call | tf_op jit(solution)/shard_map/pallas_call | solution.py:37
  96.3 9.0 %shard_map.141 = (bf16[144,512]{1,0:T(8,128)(2,1)S(1)}, bf16[144,512]{1,0:T(8,128)(2,1)S(1)}, bf16[144,512]{1,0:T(8,128)(2,1)S(1)}, bf16[144,512]{1,0:T(8,128)(2...) custom-call(s32[4]{0:T(128)S(1)} %pad_add_fusion.place.refs_0_, ...), custom_call_target="tpu_custom_call", output_to_operand_aliasing={{4}: (7, {}), {5}: (8, {})} | custom-call | tf_op jit(solution)/shard_map/pallas_call | solution.py:37
  105.5 3.3 %collective-permute-start.33 = (bf16[64,2048]{1,0:T(8,128)(2,1)S(1)}, bf16[64,2048]{1,0:T(8,128)(2,1)S(1)}, u32[]{:S(2)}, u32[]{:S(2)}) collective-permute-start(bf16[64,2048]{1,0:T(8,128)(2,1)S(1)} %slice.19), channel_id=1, source_target_pairs={{0,6},{2,0},{4,2},{6,4},{1,7},{3,1},{5,3},{7,5},{8,14},{10,8},{12,... | collective-permute-start | bytes 786440 | tf_op jit(solution)/shard_map/ppermute | solution.py:32
  108.8 4.4 %collective-permute-start.25 = (bf16[144,512]{1,0:T(8,128)(2,1)S(1)}, bf16[144,512]{1,0:T(8,128)(2,1)S(1)}, u32[]{:S(2)}, u32[]{:S(2)}) collective-permute-start(bf16[144,512]{1,0:T(8,128)(2,1)S(1)} %get-tuple-element.54), channel_id=1, source_target_pairs={{0,16},{8,24},{16,0},{24,8},{1,17},{9,25},{17,1},{25,9},{2,18},{10... | collective-permute-start | bytes 442376 | tf_op jit(solution)/shard_map/ppermute | solution.py:32
  116.3 2.0 %collective-permute-done.26.r3 = bf16[144,512]{1,0:T(8,128)(2,1)S(1)} collective-permute-done((bf16[144,512]{1,0:T(8,128)(2,1)S(1)}, bf16[144,512]{1,0:T(8,128)(2,1)S(1)}, u32[]{:S(2)}, u32[]{:S(2)}) %collective-permute-start.26) | collective-permute-done | bytes 147488 | tf_op jit(solution)/shard_map/ppermute | solution.py:32
  124.7 2.2 %collective-permute-start.36 = (bf16[64,2048]{1,0:T(8,128)(2,1)S(1)}, bf16[64,2048]{1,0:T(8,128)(2,1)S(1)}, u32[]{:S(2)}, u32[]{:S(2)}) collective-permute-start(bf16[64,2048]{1,0:T(8,128)(2,1)S(1)} %get-tuple-element.65), channel_id=1, source_target_pairs={{0,4},{2,6},{4,0},{6,2},{1,5},{3,7},{5,1},{7,3},{8,12},{10,14},{12... | collective-permute-start | bytes 786440 | tf_op jit(solution)/shard_map/ppermute | solution.py:32
  126.9 2.5 %collective-permute-start.37 = (bf16[64,2048]{1,0:T(8,128)(2,1)S(1)}, bf16[64,2048]{1,0:T(8,128)(2,1)S(1)}, u32[]{:S(2)}, u32[]{:S(2)}) collective-permute-start(bf16[64,2048]{1,0:T(8,128)(2,1)S(1)} %get-tuple-element.66), channel_id=1, source_target_pairs={{0,6},{2,0},{4,2},{6,4},{1,7},{3,1},{5,3},{7,5},{8,14},{10,8},{12,... | collective-permute-start | bytes 786440 | tf_op jit(solution)/shard_map/ppermute | solution.py:32
  130.6 5.8 %collective-permute-done.35.f1 = bf16[64,2048]{1,0:T(8,128)(2,1)S(1)} collective-permute-done((bf16[64,2048]{1,0:T(8,128)(2,1)S(1)}, bf16[64,2048]{1,0:T(8,128)(2,1)S(1)}, u32[]{:S(2)}, u32[]{:S(2)}) %collective-permute-start.35) | collective-permute-done | bytes 262176 | tf_op jit(solution)/shard_map/ppermute | solution.py:32
  (96 shorter events, 43.5 us)
Async XLA Ops:
  2.5 9.4 %collective-permute-start = (bf16[64,2048]{1,0:T(8,128)(2,1)S(1)}, bf16[64,2048]{1,0:T(8,128)(2,1)S(1)}, u32[]{:S(2)}, u32[]{:S(2)}) collective-permute-start(bf16[64,2048]{1,0:T(8,128)(2,1)S(1)} %shard_map.131.n0), channel_id=1, source_target_pairs={{0,2},{2,4},{4,6},{6,0},{1,3},{3,5},{5,7},{7,1},{8,10},{10,12},{12... | collective-permute-start | bytes 786440 | tf_op jit(solution)/shard_map/ppermute | solution.py:32
  4.1 14.5 %collective-permute-start.1 = (bf16[64,2048]{1,0:T(8,128)(2,1)S(1)}, bf16[64,2048]{1,0:T(8,128)(2,1)S(1)}, u32[]{:S(2)}, u32[]{:S(2)}) collective-permute-start(bf16[64,2048]{1,0:T(8,128)(2,1)S(1)} %shard_map.131.n0), channel_id=1, source_target_pairs={{0,4},{2,6},{4,0},{6,2},{1,5},{3,7},{5,1},{7,3},{8,12},{10,14},{12... | collective-permute-start | bytes 786440 | tf_op jit(solution)/shard_map/ppermute | solution.py:32
  7.0 11.6 %collective-permute-start.2 = (bf16[64,2048]{1,0:T(8,128)(2,1)S(1)}, bf16[64,2048]{1,0:T(8,128)(2,1)S(1)}, u32[]{:S(2)}, u32[]{:S(2)}) collective-permute-start(bf16[64,2048]{1,0:T(8,128)(2,1)S(1)} %shard_map.131.n0), channel_id=1, source_target_pairs={{0,6},{2,0},{4,2},{6,4},{1,7},{3,1},{5,3},{7,5},{8,14},{10,8},{12,... | collective-permute-start | bytes 786440 | tf_op jit(solution)/shard_map/ppermute | solution.py:32
  8.4 16.9 %collective-permute-start.3 = (bf16[64,2048]{1,0:T(8,128)(2,1)S(1)}, bf16[64,2048]{1,0:T(8,128)(2,1)S(1)}, u32[]{:S(2)}, u32[]{:S(2)}) collective-permute-start(bf16[64,2048]{1,0:T(8,128)(2,1)S(1)} %shard_map.131.n0), channel_id=1, source_target_pairs={{0,1},{1,0},{2,3},{3,2},{4,5},{5,4},{6,7},{7,6},{8,9},{9,8},{10,11... | collective-permute-start | bytes 786440 | tf_op jit(solution)/shard_map/ppermute | solution.py:32
  11.9 13.5 %collective-permute-start.4 = (bf16[64,2048]{1,0:T(8,128)(2,1)S(1)}, bf16[64,2048]{1,0:T(8,128)(2,1)S(1)}, u32[]{:S(2)}, u32[]{:S(2)}) collective-permute-start(bf16[64,2048]{1,0:T(8,128)(2,1)S(1)} %collective-permute-done.n1), channel_id=1, source_target_pairs={{0,1},{1,0},{2,3},{3,2},{4,5},{5,4},{6,7},{7,6},{8,9},{9,8},{10,11... | collective-permute-start | bytes 786440 | tf_op jit(solution)/shard_map/ppermute | solution.py:32
  28.4 8.3 %collective-permute-start.16 = (bf16[1024,128]{1,0:T(8,128)(2,1)S(1)}, bf16[1024,128]{1,0:T(8,128)(2,1)S(1)}, u32[]{:S(2)}, u32[]{:S(2)}) collective-permute-start(bf16[1024,128]{1,0:T(8,128)(2,1)S(1)} %get-tuple-element.43.kv), channel_id=1, source_target_pairs={{0,32},{32,64},{64,96},{96,128},{128,160},{160,192},{192,224},{224... | collective-permute-start | bytes 786440 | tf_op jit(solution)/shard_map/ppermute | solution.py:32
  28.5 9.7 %collective-permute-start.20 = (bf16[1024,128]{1,0:T(8,128)(2,1)S(1)}, bf16[1024,128]{1,0:T(8,128)(2,1)S(1)}, u32[]{:S(2)}, u32[]{:S(2)}) collective-permute-start(bf16[1024,128]{1,0:T(8,128)(2,1)S(1)} %get-tuple-element.43.kv), channel_id=1, source_target_pairs={{0,224},{32,0},{64,32},{96,64},{128,96},{160,128},{192,160},{224,1... | collective-permute-start | bytes 786440 | tf_op jit(solution)/shard_map/ppermute | solution.py:32
  36.7 25.5 %collective-permute-start.17 = (bf16[1024,128]{1,0:T(8,128)(2,1)S(1)}, bf16[1024,128]{1,0:T(8,128)(2,1)S(1)}, u32[]{:S(2)}, u32[]{:S(2)}) collective-permute-start(bf16[1024,128]{1,0:T(8,128)(2,1)S(1)} %collective-permute-done.16.refs_3_), channel_id=1, source_target_pairs={{0,32},{32,64},{64,96},{96,128},{128,160},{160,192},{192,224},{224... | collective-permute-start | bytes 786440 | tf_op jit(solution)/shard_map/ppermute | solution.py:32
  38.2 24.0 %collective-permute-start.21 = (bf16[1024,128]{1,0:T(8,128)(2,1)S(1)}, bf16[1024,128]{1,0:T(8,128)(2,1)S(1)}, u32[]{:S(2)}, u32[]{:S(2)}) collective-permute-start(bf16[1024,128]{1,0:T(8,128)(2,1)S(1)} %collective-permute-done.20.refs_4_), channel_id=1, source_target_pairs={{0,224},{32,0},{64,32},{96,64},{128,96},{160,128},{192,160},{224,1... | collective-permute-start | bytes 786440 | tf_op jit(solution)/shard_map/ppermute | solution.py:32
  58.8 62.8 %collective-permute-start.12 = (bf16[4,64,2048]{2,1,0:T(8,128)(2,1)S(1)}, bf16[4,64,2048]{2,1,0:T(8,128)(2,1)S(1)}, u32[]{:S(2)}, u32[]{:S(2)}) collective-permute-start(bf16[4,64,2048]{2,1,0:T(8,128)(2,1)S(1)} %get-tuple-element.40), channel_id=1, source_target_pairs={{0,1},{1,0},{2,3},{3,2},{4,5},{5,4},{6,7},{7,6},{8,9},{9,8},{10,11... | collective-permute-start | bytes 3145736 | tf_op jit(solution)/shard_map/ppermute | solution.py:32
  62.2 8.4 %collective-permute-start.18 = (bf16[1024,128]{1,0:T(8,128)(2,1)S(1)}, bf16[1024,128]{1,0:T(8,128)(2,1)S(1)}, u32[]{:S(2)}, u32[]{:S(2)}) collective-permute-start(bf16[1024,128]{1,0:T(8,128)(2,1)S(1)} %collective-permute-done.17.refs_3_), channel_id=1, source_target_pairs={{0,32},{32,64},{64,96},{96,128},{128,160},{160,192},{192,224},{224... | collective-permute-start | bytes 786440 | tf_op jit(solution)/shard_map/ppermute | solution.py:32
  62.2 9.6 %collective-permute-start.22 = (bf16[1024,128]{1,0:T(8,128)(2,1)S(1)}, bf16[1024,128]{1,0:T(8,128)(2,1)S(1)}, u32[]{:S(2)}, u32[]{:S(2)}) collective-permute-start(bf16[1024,128]{1,0:T(8,128)(2,1)S(1)} %collective-permute-done.21.refs_4_), channel_id=1, source_target_pairs={{0,224},{32,0},{64,32},{96,64},{128,96},{160,128},{192,160},{224,1... | collective-permute-start | bytes 786440 | tf_op jit(solution)/shard_map/ppermute | solution.py:32
  64.3 41.1 %collective-permute-start.30 = (bf16[128,2048]{1,0:T(8,128)(2,1)S(1)}, bf16[128,2048]{1,0:T(8,128)(2,1)S(1)}, u32[]{:S(2)}, u32[]{:S(2)}) collective-permute-start(bf16[128,2048]{1,0:T(8,128)(2,1)S(1)} %copy-done.6), channel_id=1, source_target_pairs={{0,2},{2,4},{4,6},{6,0},{1,3},{3,5},{5,7},{7,1},{8,10},{10,12},{12... | collective-permute-start | bytes 1572872 | tf_op jit(solution)/shard_map/ppermute | solution.py:32
  65.6 39.9 %collective-permute-start.32 = (bf16[128,2048]{1,0:T(8,128)(2,1)S(1)}, bf16[128,2048]{1,0:T(8,128)(2,1)S(1)}, u32[]{:S(2)}, u32[]{:S(2)}) collective-permute-start(bf16[128,2048]{1,0:T(8,128)(2,1)S(1)} %copy-done.6), channel_id=1, source_target_pairs={{0,6},{2,0},{4,2},{6,4},{1,7},{3,1},{5,3},{7,5},{8,14},{10,8},{12,... | collective-permute-start | bytes 1572872 | tf_op jit(solution)/shard_map/ppermute | solution.py:32
  71.9 8.1 %collective-permute-start.15 = (bf16[128,512]{1,0:T(8,128)(2,1)S(1)}, bf16[128,512]{1,0:T(8,128)(2,1)S(1)}, u32[]{:S(2)}, u32[]{:S(2)}) collective-permute-start(bf16[128,512]{1,0:T(8,128)(2,1)S(1)} %get-tuple-element.42.q0), channel_id=1, source_target_pairs={{0,24},{8,0},{16,8},{24,16},{1,25},{9,1},{17,9},{25,17},{2,26},{10... | collective-permute-start | bytes 393224 | tf_op jit(solution)/shard_map/ppermute | solution.py:32
  78.2 18.1 %collective-permute-start.19 = (bf16[512,128]{1,0:T(8,128)(2,1)S(1)}, bf16[512,128]{1,0:T(8,128)(2,1)S(1)}, u32[]{:S(2)}, u32[]{:S(2)}) collective-permute-start(bf16[512,128]{1,0:T(8,128)(2,1)S(1)} %slice.16), channel_id=1, source_target_pairs={{0,32},{32,64},{64,96},{96,128},{128,160},{160,192},{192,224},{224... | collective-permute-start | bytes 393224 | tf_op jit(solution)/shard_map/ppermute | solution.py:32
  80.0 16.3 %collective-permute-start.23 = (bf16[512,128]{1,0:T(8,128)(2,1)S(1)}, bf16[512,128]{1,0:T(8,128)(2,1)S(1)}, u32[]{:S(2)}, u32[]{:S(2)}) collective-permute-start(bf16[512,128]{1,0:T(8,128)(2,1)S(1)} %slice.17), channel_id=1, source_target_pairs={{0,224},{32,0},{64,32},{96,64},{128,96},{160,128},{192,160},{224,1... | collective-permute-start | bytes 393224 | tf_op jit(solution)/shard_map/ppermute | solution.py:32
  105.3 7.9 %collective-permute-start.24 = (bf16[144,512]{1,0:T(8,128)(2,1)S(1)}, bf16[144,512]{1,0:T(8,128)(2,1)S(1)}, u32[]{:S(2)}, u32[]{:S(2)}) collective-permute-start(bf16[144,512]{1,0:T(8,128)(2,1)S(1)} %get-tuple-element.53), channel_id=1, source_target_pairs={{0,24},{8,0},{16,8},{24,16},{1,25},{9,1},{17,9},{25,17},{2,26},{10... | collective-permute-start | bytes 442376 | tf_op jit(solution)/shard_map/ppermute | solution.py:32
  105.4 18.4 %collective-permute-start.31 = (bf16[64,2048]{1,0:T(8,128)(2,1)S(1)}, bf16[64,2048]{1,0:T(8,128)(2,1)S(1)}, u32[]{:S(2)}, u32[]{:S(2)}) collective-permute-start(bf16[64,2048]{1,0:T(8,128)(2,1)S(1)} %slice.18), channel_id=1, source_target_pairs={{0,2},{2,4},{4,6},{6,0},{1,3},{3,5},{5,7},{7,1},{8,10},{10,12},{12... | collective-permute-start | bytes 786440 | tf_op jit(solution)/shard_map/ppermute | solution.py:32
  105.5 19.2 %collective-permute-start.33 = (bf16[64,2048]{1,0:T(8,128)(2,1)S(1)}, bf16[64,2048]{1,0:T(8,128)(2,1)S(1)}, u32[]{:S(2)}, u32[]{:S(2)}) collective-permute-start(bf16[64,2048]{1,0:T(8,128)(2,1)S(1)} %slice.19), channel_id=1, source_target_pairs={{0,6},{2,0},{4,2},{6,4},{1,7},{3,1},{5,3},{7,5},{8,14},{10,8},{12,... | collective-permute-start | bytes 786440 | tf_op jit(solution)/shard_map/ppermute | solution.py:32
  119.8 9.7 %collective-permute-start.28 = (bf16[128,128]{1,0:T(8,128)(2,1)S(1)}, bf16[128,128]{1,0:T(8,128)(2,1)S(1)}, u32[]{:S(2)}, u32[]{:S(2)}) collective-permute-start(bf16[128,128]{1,0:T(8,128)(2,1)S(1)} %get-tuple-element.59), channel_id=1, source_target_pairs={{0,4},{2,6},{4,0},{6,2},{1,5},{3,7},{5,1},{7,3},{8,12},{10,14},{12... | collective-permute-start | bytes 98312 | tf_op jit(solution)/shard_map/ppermute | solution.py:32
  123.8 12.7 %collective-permute-start.35 = (bf16[64,2048]{1,0:T(8,128)(2,1)S(1)}, bf16[64,2048]{1,0:T(8,128)(2,1)S(1)}, u32[]{:S(2)}, u32[]{:S(2)}) collective-permute-start(bf16[64,2048]{1,0:T(8,128)(2,1)S(1)} %get-tuple-element.64), channel_id=1, source_target_pairs={{0,2},{2,4},{4,6},{6,0},{1,3},{3,5},{5,7},{7,1},{8,10},{10,12},{12... | collective-permute-start | bytes 786440 | tf_op jit(solution)/shard_map/ppermute | solution.py:32
  124.7 11.7 %collective-permute-start.36 = (bf16[64,2048]{1,0:T(8,128)(2,1)S(1)}, bf16[64,2048]{1,0:T(8,128)(2,1)S(1)}, u32[]{:S(2)}, u32[]{:S(2)}) collective-permute-start(bf16[64,2048]{1,0:T(8,128)(2,1)S(1)} %get-tuple-element.65), channel_id=1, source_target_pairs={{0,4},{2,6},{4,0},{6,2},{1,5},{3,7},{5,1},{7,3},{8,12},{10,14},{12... | collective-permute-start | bytes 786440 | tf_op jit(solution)/shard_map/ppermute | solution.py:32
  126.9 10.4 %collective-permute-start.37 = (bf16[64,2048]{1,0:T(8,128)(2,1)S(1)}, bf16[64,2048]{1,0:T(8,128)(2,1)S(1)}, u32[]{:S(2)}, u32[]{:S(2)}) collective-permute-start(bf16[64,2048]{1,0:T(8,128)(2,1)S(1)} %get-tuple-element.66), channel_id=1, source_target_pairs={{0,6},{2,0},{4,2},{6,4},{1,7},{3,1},{5,3},{7,5},{8,14},{10,8},{12,... | collective-permute-start | bytes 786440 | tf_op jit(solution)/shard_map/ppermute | solution.py:32
  (26 other events, 259.3 us)
where the time goes:
time: 141 us; the launch traced here: 138 us
  waiting for transfers between devices  47.4 us (34%)
  starting transfers between devices  45.7 us (32%)
  Pallas kernels  36.7 us (26%)
  local copies, waits for them, and re-layouts  7.29 us (5%)
    ppermute x37, starting transfers between devices, turn(): return lax.ppermute(array, axis, [(i, (i + by) % n) for i in range(n)])  44.4 us
    ppermute x37, waiting for transfers between devices, turn(): return lax.ppermute(array, axis, [(i, (i + by) % n) for i in range(n)])  43.1 us
    pallas_call x14, Pallas kernels, kernel(): pl.pallas_call(body, out_shape=outs, in_specs=[sspec()] * scalars + [spec...  36.7 us
    unnamed x24, local copies, waits for them, and re-layouts  7.23 us
    ppermute x1, waiting for transfers between devices, per_device(): rim = lax.ppermute(rim, ('z', 'x'), [(i, i + 1) for i in range(31)])  4.33 us
  transfers between devices with their start and end apart: 38, of which 16 were waited for; matrix products, arithmetic and copies ran while one was open for 0% of the time, Pallas kernels for 24%

commit v1 on v0

--- a/solution.py
+++ b/solution.py
@@ -16,7 +16,7 @@
 BF16 = jnp.bfloat16
 VMEM = pltpu.MemorySpace.VMEM
 SMEM = pltpu.MemorySpace.SMEM
-PARAMS = pltpu.CompilerParams(vmem_limit_bytes=24 * 2**20)
+PARAMS = pltpu.CompilerParams(vmem_limit_bytes=20 * 2**20)
 
 
 def vspec():
@@ -32,12 +32,20 @@
     return lax.ppermute(array, axis, [(i, (i + by) % n) for i in range(n)])
 
 
-def kernel(body, outs, args, scratch=(), aliases=None, scalars=1, far=False):
-    spec = pl.BlockSpec(memory_space=pltpu.MemorySpace.HBM) if far else vspec()
+def swap(array, axis, bit):
+    n = lax.axis_size(axis)
+    return lax.ppermute(array, axis, [(i, i ^ bit) for i in range(n)])
+
+
+def kernel(body, outs, args, scratch=(), aliases=None, scalars=1, far=0):
+    hbm = pltpu.MemorySpace.HBM
+    near = len(args) - far
+    args = (*args[:near], *(pltpu.with_memory_space_constraint(a, hbm) for a in args[near:]))
+    specs = [sspec()] * scalars + [vspec()] * (near - scalars)
     return pl.pallas_call(
         body,
         out_shape=outs,
-        in_specs=[sspec()] * scalars + [spec] * (len(args) - scalars),
+        in_specs=specs + [pl.BlockSpec(memory_space=hbm)] * far,
         out_specs=jax.tree.map(lambda _: vspec(), outs),
         scratch_shapes=list(scratch),
         input_output_aliases=aliases or {},
@@ -49,15 +57,11 @@
     return jax.ShapeDtypeStruct(dims, dtype)
 
 
-def after(x, other):
-    return lax.optimization_barrier((x, other))[0]
-
-
 WIDTHS = (128, 128, 128, 256, 256)
 
 
 def load_body(*refs):
-    weights, out, sems = refs[:5], refs[5], refs[6]
+    weights, out, sems = refs[1:6], refs[6], refs[7]
     copies, at = [], 0
     for k, (ref, width) in enumerate(zip(weights, WIDTHS)):
         copies.append(pltpu.make_async_copy(ref, out.at[:, at : at + width], sems.at[k]))
@@ -143,61 +147,31 @@
     lax.fori_loop(0, 4, block, 0)
 
 
-def gate_body(place, convolved, s0, s1, s2, s3, gain, weights, mine, theirs, left):
-    c = place[1]
-    square = (s0[...] + s1[...] + s2[...] + s3[...]) / 2048.0
+def gate_body(place, convolved, total, gain, weights, g0, g1, g2, g3, left):
+    y = place[0]
+    square = total[...] / 2048.0
     column = jnp.transpose(jnp.broadcast_to(lax.rsqrt(square + 1e-06), (128, 512)))
     factor = jnp.concatenate([column, column], axis=1)
     v = convolved[...] * factor * gain[...]
     left[...] = (v / (1.0 + jnp.exp(-v))).astype(BF16)
-
-    def block(y, carry):
-        rows = left[pl.ds(pl.multiple_of(128 * y, 128), 128), :]
-        part = jnp.dot(rows, weights[...], preferred_element_type=F32).astype(BF16)
-
-        @pl.when(c == 0)
-        def _():
-            mine[y] = part[:64]
-            theirs[y] = part[64:]
-
-        @pl.when(c == 1)
-        def _():
-            mine[y] = part[64:]
-            theirs[y] = part[:64]
-
-        return carry
-
-    lax.fori_loop(0, 4, block, 0)
-
-
-def fold_body(place, mine, theirs, own, f1, f2, f3):
-    y = place[0]
-    for k, ref in enumerate((own, f1, f2, f3)):
-        at = lax.rem(y + k, 4)
-        total = mine[at].astype(F32) + theirs[at].astype(F32)
-        ref[...] = total.astype(ref.dtype)
-
-
-def part_body(place, own, h0, h1, h2, h3, w0, w1, w2a, w2b, w3, mine, theirs):
+    for k, out in enumerate((g0, g1, g2, g3)):
+        at = pl.multiple_of(lax.rem(y + k, 4) * 128, 128)
+        rows = left[pl.ds(at, 128), :]
+        out[...] = jnp.dot(rows, weights[...], preferred_element_type=F32).astype(BF16)
+
+
+def part_body(place, h0, h1, h2, h3, g0, g1, g2, g3, w0, w1, w2, w3, mine, theirs, both):
     c = place[1]
     left = jnp.concatenate([h0[...], h1[...], h2[...], h3[...]], axis=1)
-    right = jnp.concatenate([w0[...], w1[...], w2a[...], w2b[...], w3[...]], axis=0)
-    both = jnp.dot(left, right, preferred_element_type=F32)
-
-    @pl.when(c == 0)
-    def _():
-        mine[...] = both[:64] + own[...]
-        theirs[...] = both[64:].astype(BF16)
-
-    @pl.when(c == 1)
-    def _():
-        mine[...] = both[64:] + own[...]
-        theirs[...] = both[:64].astype(BF16)
-
-
-def final_body(mine, theirs, f1, f2, f3, out):
-    folded = f1[...].astype(F32) + f2[...].astype(F32) + f3[...].astype(F32)
-    out[...] = (mine[...] + theirs[...].astype(F32) + folded).astype(BF16)
+    right = jnp.concatenate([w0[...], w1[...], w2[...], w3[...]], axis=0)
+    conv = g0[...].astype(F32) + g1[...].astype(F32) + g2[...].astype(F32) + g3[...].astype(F32)
+    both[...] = jnp.dot(left, right, preferred_element_type=F32) + conv
+    mine[...] = both[pl.ds(pl.multiple_of(c * 64, 64), 64), :]
+    theirs[...] = both[pl.ds(pl.multiple_of((1 - c) * 64, 64), 64), :].astype(BF16)
+
+
+def final_body(mine, theirs, out):
+    out[...] = (mine[...] + theirs[...].astype(F32)).astype(BF16)
 
 
 DEPTH = 4
@@ -322,7 +296,7 @@
 
 def more_body(shifts, last, place, q, bias, *refs):
     n = len(shifts)
-    m = n + last
+    m = n
     blocks = refs[:m]
     if last:
         outs = refs[m + 2 : m + 6]
@@ -342,14 +316,8 @@
 
     @pl.when(count > 0)
     def _():
-        if last:
-            kvs[0] = blocks[0][...]
-            kvs[1, :512] = blocks[1][...]
-            kvs[1, 512:] = blocks[2][...]
-            kvs[2] = blocks[3][...]
-        else:
-            for k, ref in enumerate(blocks):
-                kvs[k] = ref[...]
+        for k, ref in enumerate(blocks):
+            kvs[k] = ref[...]
 
         def block(i):
             return i // 2 if isinstance(i, int) else lax.shift_right_logical(i, 1)
@@ -392,9 +360,6 @@
     def body(*refs):
         more_body(shifts, last, *refs)
 
-    if last:
-        first, (upper, lower), third = kvs
-        kvs = (first, upper, lower, third)
     n = len(kvs)
     outs = (shape(144, 512),) * 4 if last else ()
     aliases = {3 + n: len(outs), 4 + n: len(outs) + 1}
@@ -456,21 +421,23 @@
             pltpu.SemaphoreType.DMA((2,)),
         ],
         scalars=0,
-        far=True,
+        far=2,
     )
     own = [n0] + [turn(n0, "y", k) for k in (1, 2, 3)]
     partner = [turn(piece, "c", 1) for piece in own]
 
+    ws = [out_attn] + [turn(out_attn, "y", k) for k in (1, 2, 3)]
+
+    bias, cum_own = kernel(
+        bias_body, (shape(8, 512, 128), shape(2, 512, dtype=F32)), (place, cum_gate)
+    )
     weights = kernel(
         load_body,
         shape(2048, 896),
-        (w_query, w_key, w_value, conv_in, conv_gate),
+        (cum_own, w_query, w_key, w_value, conv_in, conv_gate),
         [pltpu.SemaphoreType.DMA((5,))],
         scalars=0,
-        far=True,
-    )
-    bias, cum_own = kernel(
-        bias_body, (shape(8, 512, 128), shape(2, 512, dtype=F32)), (place, cum_gate)
+        far=5,
     )
 
     qT, kv, gated, rim = kernel(
@@ -488,8 +455,7 @@
     b2 = turn(b1, "z", -1)
     a3 = turn(a2, "z", 1)
     b3 = turn(b2, "z", -1)
-    fa = turn(a3[:512], "z", 1)
-    fb = turn(b3[512:], "z", -1)
+    a4 = turn(a3, "z", 1)
 
     convolved, square = kernel(
         conv_body,
@@ -499,29 +465,20 @@
         scalars=0,
     )
     square = square + turn(square, "c", 1)
-    squares = [square] + [turn(square, "y", k) for k in (1, 2, 3)]
-    mine, theirs = kernel(
+    square = square + swap(square, "y", 1)
+    square = square + swap(square, "y", 2)
+    parts = kernel(
         gate_body,
-        (shape(4, 64, 2048), shape(4, 64, 2048)),
-        (place, convolved, *squares, conv_gain[None, :], out_conv),
+        (shape(128, 2048),) * 4,
+        (place, convolved, square, conv_gain[None, :], out_conv),
         [pltpu.VMEM((512, 256), BF16)],
     )
-    theirs = turn(theirs, "c", 1)
-    folded = kernel(
-        fold_body, (shape(64, 2048, dtype=F32),) + (shape(64, 2048),) * 3, (place, mine, theirs)
-    )
-    folded = [folded[0]] + [turn(folded[k], "y", k) for k in (1, 2, 3)]
-
-    w0 = after(out_attn, kv)
-    w1 = turn(w0, "y", 1)
-    w3 = turn(w0, "y", 3)
-    w2a = turn(w1[:64], "y", 1)
-    w2b = turn(w3[64:], "y", 3)
+    parts = [parts[0]] + [turn(parts[k], "y", k) for k in (1, 2, 3)]
 
     *state, q = attend_first(place, qs, kv, bias)
     state = attend_more(place, q, bias, (a1, b1), (1, -1), state)
     state = attend_more(place, q, bias, (a2, b2), (2, -2), state)
-    outs = attend_more(place, q, bias, (a3, (fa, fb), b3), (3, 4, -3), state, True)
+    outs = attend_more(place, q, bias, (a3, a4, b3), (3, 4, -3), state, True)
     others = [turn(outs[k], "x", -k) for k in (1, 2, 3)]
     log_total, *pieces = kernel(
         merge_body,
@@ -533,10 +490,11 @@
     mine, theirs = kernel(
         part_body,
         (shape(64, 2048, dtype=F32), shape(64, 2048)),
-        (place, folded[0], *heads, w0, w1, w2a, w2b, w3),
+        (place, *heads, *parts, *ws),
+        [pltpu.VMEM((128, 2048), F32)],
     )
     theirs = turn(theirs, "c", 1)
-    mixed = kernel(final_body, shape(64, 2048), (mine, theirs, *folded[1:]), scalars=0)
+    mixed = kernel(final_body, shape(64, 2048), (mine, theirs), scalars=0)
     return (mixed, log_total)
 
 

time: 141 us -> 161 us (1.14)
  waiting for transfers between devices: 47.4 us -> 73.4 us
  local copies, waits for them, and re-layouts: 7.29 us -> 0.93 us
    ppermute x37 -> x31, waiting for transfers between devices: 43.1 us -> 65.8 us  [turn(): return lax.ppermute(array, axis, [(i, (i + by) % n) for i in range(n)])]
    unnamed x24 -> x10, local copies, waits for them, and re-layouts: 7.23 us -> 0.93 us
    ppermute x0 -> x2, starting transfers between devices: none -> 5.56 us  [swap(): return lax.ppermute(array, axis, [(i, i ^ bit) for i in range(n)])]
    ppermute x37 -> x31, starting transfers between devices: 44.4 us -> 39.7 us  [turn(): return lax.ppermute(array, axis, [(i, (i + by) % n) for i in range(n)])]
    ppermute x0 -> x2, waiting for transfers between devices: none -> 3.31 us  [swap(): return lax.ppermute(array, axis, [(i, i ^ bit) for i in range(n)])]
    pallas_call x14 -> x13, Pallas kernels: 36.7 us -> 37.5 us  [kernel(): pl.pallas_call(body, out_shape=outs, in_specs=specs + [pl.BlockSpec(memor...]
  transfers between devices with their start and end apart: 38 -> 34, of which waited for: 16 -> 18; matrix products, arithmetic and copies ran while one was open for 0% -> 0% of each run, Pallas kernels for 24% -> 20%
where the time goes in v1:
time: 161 us; the launch traced here: 159 us
  waiting for transfers between devices  73.4 us (46%)
  starting transfers between devices  46.5 us (29%)
  Pallas kernels  37.5 us (23%)
    ppermute x31, waiting for transfers between devices, turn(): return lax.ppermute(array, axis, [(i, (i + by) % n) for i in range(n)])  65.8 us
    ppermute x31, starting transfers between devices, turn(): return lax.ppermute(array, axis, [(i, (i + by) % n) for i in range(n)])  39.7 us
    pallas_call x13, Pallas kernels, kernel(): pl.pallas_call(body, out_shape=outs, in_specs=specs + [pl.BlockSpec(memor...  37.5 us
    ppermute x2, starting transfers between devices, swap(): return lax.ppermute(array, axis, [(i, i ^ bit) for i in range(n)])  5.56 us
    ppermute x1, waiting for transfers between devices, per_device(): rim = lax.ppermute(rim, ('z', 'x'), [(i, i + 1) for i in range(31)])  4.33 us
    ppermute x2, waiting for transfers between devices, swap(): return lax.ppermute(array, axis, [(i, i ^ bit) for i in range(n)])  3.31 us
  transfers between devices with their start and end apart: 34, of which 18 were waited for; matrix products, arithmetic and copies ran while one was open for 0% of the time, Pallas kernels for 20%

profile of v1, /device:TPU:230, one launch (start us, length us, event | category | flops | bytes accessed | tf_op | source)
XLA Modules:
  0.0 159.3 jit_solution(2781651851815715894)
XLA Ops:
  3.4 2.9 %collective-permute-start.1 = (bf16[64,2048]{1,0:T(8,128)(2,1)S(1)}, bf16[64,2048]{1,0:T(8,128)(2,1)S(1)}, u32[]{:S(2)}, u32[]{:S(2)}) collective-permute-start(bf16[64,2048]{1,0:T(8,128)(2,1)S(1)} %shard_map.131.n0), channel_id=1, source_target_pairs={{0,4},{2,6},{4,0},{6,2},{1,5},{3,7},{5,1},{7,3},{8,12},{10,14},{12... | collective-permute-start | bytes 786440 | tf_op jit(solution)/shard_map/ppermute | solution.py:32
  7.7 3.5 %collective-permute-done.n1 = bf16[64,2048]{1,0:T(8,128)(2,1)S(1)} collective-permute-done((bf16[64,2048]{1,0:T(8,128)(2,1)S(1)}, bf16[64,2048]{1,0:T(8,128)(2,1)S(1)}, u32[]{:S(2)}, u32[]{:S(2)}) %collective-permute-start) | collective-permute-done | bytes 262176 | tf_op jit(solution)/shard_map/ppermute | solution.py:32
  11.2 6.8 %collective-permute-done.1.n2 = bf16[64,2048]{1,0:T(8,128)(2,1)S(1)} collective-permute-done((bf16[64,2048]{1,0:T(8,128)(2,1)S(1)}, bf16[64,2048]{1,0:T(8,128)(2,1)S(1)}, u32[]{:S(2)}, u32[]{:S(2)}) %collective-permute-start.1) | collective-permute-done | bytes 262176 | tf_op jit(solution)/shard_map/ppermute | solution.py:32
  22.6 3.0 %shard_map.134 = (bf16[128,512]{1,0:T(8,128)(2,1)S(1)}, bf16[1024,128]{1,0:T(8,128)(2,1)S(1)}, bf16[512,256]{1,0:T(8,128)(2,1)S(1)}, bf16[32,256]{1,0:T(8,128)(2,1)S(1)}) custom-call(s32[4]{0:T(128)S(1)} %pad_add_fusion.place.refs_0_, bf16[64,2048]{1,0:T(8,128)(2,1)S(1)} %shard_map.131.n0, bf16[64,2048]{1,0:T(8,128)(2,1)S(1)} %collective-permute-done.n1, ...), custom_call_target="tpu_custom_call" | custom-call | tf_op jit(solution)/shard_map/pallas_call | solution.py:45
  27.7 6.2 %collective-permute-done.10.refs_3_ = bf16[1024,128]{1,0:T(8,128)(2,1)S(1)} collective-permute-done((bf16[1024,128]{1,0:T(8,128)(2,1)S(1)}, bf16[1024,128]{1,0:T(8,128)(2,1)S(1)}, u32[]{:S(2)}, u32[]{:S(2)}) %collective-permute-start.10) | collective-permute-done | bytes 262176 | tf_op jit(solution)/shard_map/ppermute | solution.py:32
  35.9 5.3 %collective-permute-done.11.refs_3_ = bf16[1024,128]{1,0:T(8,128)(2,1)S(1)} collective-permute-done((bf16[1024,128]{1,0:T(8,128)(2,1)S(1)}, bf16[1024,128]{1,0:T(8,128)(2,1)S(1)}, u32[]{:S(2)}, u32[]{:S(2)}) %collective-permute-start.11) | collective-permute-done | bytes 262176 | tf_op jit(solution)/shard_map/ppermute | solution.py:32
  41.2 3.0 %collective-permute-start.12 = (bf16[1024,128]{1,0:T(8,128)(2,1)S(1)}, bf16[1024,128]{1,0:T(8,128)(2,1)S(1)}, u32[]{:S(2)}, u32[]{:S(2)}) collective-permute-start(bf16[1024,128]{1,0:T(8,128)(2,1)S(1)} %collective-permute-done.11.refs_3_), channel_id=1, source_target_pairs={{0,32},{32,64},{64,96},{96,128},{128,160},{160,192},{192,224},{224... | collective-permute-start | bytes 786440 | tf_op jit(solution)/shard_map/ppermute | solution.py:32
  48.5 3.7 %collective-permute-start.13 = (bf16[1024,128]{1,0:T(8,128)(2,1)S(1)}, bf16[1024,128]{1,0:T(8,128)(2,1)S(1)}, u32[]{:S(2)}, u32[]{:S(2)}) collective-permute-start(bf16[1024,128]{1,0:T(8,128)(2,1)S(1)} %collective-permute-done.12.refs_3_), channel_id=1, source_target_pairs={{0,32},{32,64},{64,96},{96,128},{128,160},{160,192},{192,224},{224... | collective-permute-start | bytes 786440 | tf_op jit(solution)/shard_map/ppermute | solution.py:32
  53.6 5.1 %collective-permute-done.8.q2 = bf16[128,512]{1,0:T(8,128)(2,1)S(1)} collective-permute-done((bf16[128,512]{1,0:T(8,128)(2,1)S(1)}, bf16[128,512]{1,0:T(8,128)(2,1)S(1)}, u32[]{:S(2)}, u32[]{:S(2)}) %collective-permute-start.8) | collective-permute-done | bytes 131104 | tf_op jit(solution)/shard_map/ppermute | solution.py:32
  62.0 6.2 %shard_map.136 = (f32[4,2,80,512]{3,2,1,0:T(8,128)S(1)}, f32[4,2,1,512]{3,2,1,0:T(1,128)S(1)}) custom-call(s32[4]{0:T(128)S(1)} %pad_add_fusion.place.refs_0_, bf16[4,128,512]{2,1,0:T(8,128)(2,1)S(1)} %get-tuple-element.36.refs_1_, bf16[8,512,128]{2,1,0:T(8,128)(2,1)S(1)} %get-tuple-element.35.bias.refs_2_, ...), custom_call_target="tpu_custom_call", output_to_operand_aliasing={{0}: (5, {}), {1}: (6, {})} | custom-call | tf_op jit(solution)/shard_map/pallas_call | solution.py:45
  68.2 6.2 %shard_map.137 = (f32[4,2,80,512]{3,2,1,0:T(8,128)S(1)}, f32[4,2,1,512]{3,2,1,0:T(1,128)S(1)}) custom-call(s32[4]{0:T(128)S(1)} %pad_add_fusion.place.refs_0_, bf16[4,128,512]{2,1,0:T(8,128)(2,1)S(1)} %get-tuple-element.36.refs_1_, bf16[8,512,128]{2,1,0:T(8,128)(2,1)S(1)} %get-tuple-element.35.bias.refs_2_, ...), custom_call_target="tpu_custom_call", output_to_operand_aliasing={{0}: (5, {}), {1}: (6, {})} | custom-call | tf_op jit(solution)/shard_map/pallas_call | solution.py:45
  74.4 9.0 %shard_map.138 = (bf16[144,512]{1,0:T(8,128)(2,1)S(1)}, bf16[144,512]{1,0:T(8,128)(2,1)S(1)}, bf16[144,512]{1,0:T(8,128)(2,1)S(1)}, bf16[144,512]{1,0:T(8,128)(2...) custom-call(s32[4]{0:T(128)S(1)} %pad_add_fusion.place.refs_0_, ...), custom_call_target="tpu_custom_call", output_to_operand_aliasing={{4}: (6, {}), {5}: (7, {})} | custom-call | tf_op jit(solution)/shard_map/pallas_call | solution.py:45
  84.2 3.7 %collective-permute-start.18 = (bf16[144,512]{1,0:T(8,128)(2,1)S(1)}, bf16[144,512]{1,0:T(8,128)(2,1)S(1)}, u32[]{:S(2)}, u32[]{:S(2)}) collective-permute-start(bf16[144,512]{1,0:T(8,128)(2,1)S(1)} %get-tuple-element.45), channel_id=1, source_target_pairs={{0,16},{8,24},{16,0},{24,8},{1,17},{9,25},{17,1},{25,9},{2,18},{10... | collective-permute-start | bytes 442376 | tf_op jit(solution)/shard_map/ppermute | solution.py:32
  90.4 4.3 %collective-permute-done.23.rim = bf16[32,256]{1,0:T(8,128)(2,1)S(1)} collective-permute-done((bf16[32,256]{1,0:T(8,128)(2,1)S(1)}, bf16[32,256]{1,0:T(8,128)(2,1)S(1)}, u32[]{:S(2)}, u32[]{:S(2)}) %collective-permute-start.23) | collective-permute-done | bytes 16416 | tf_op jit(solution)/shard_map/ppermute | solution.py:450
  94.7 2.2 %shard_map.140 = (f32[512,256]{1,0:T(8,128)S(1)}, f32[1,512]{1,0:T(1,128)S(1)}) custom-call(bf16[512,256]{1,0:T(8,128)(2,1)S(1)} %get-tuple-element.51.gated, bf16[32,256]{1,0:T(8,128)(2,1)S(1)} %collective-permute-done.23.rim, f32[31,256]{1,0:T(8,128)S(1)} %copy-done.3), custom_call_target="tpu_custom_call" | custom-call | tf_op jit(solution)/shard_map/pallas_call | solution.py:45
  102.0 3.3 %collective-permute-start.26 = (f32[1,512]{1,0:T(1,128)S(1)}, f32[1,512]{1,0:T(1,128)S(1)}, u32[]{:S(2)}, u32[]{:S(2)}) collective-permute-start(f32[1,512]{1,0:T(1,128)S(1)} %add.10), channel_id=1, source_target_pairs={{0,4},{2,6},{4,0},{6,2},{1,5},{3,7},{5,1},{7,3},{8,12},{10,14},{12... | collective-permute-start | bytes 6152 | tf_op jit(solution)/shard_map/ppermute | solution.py:37
  107.1 3.3 %collective-permute-start.31 = (bf16[128,2048]{1,0:T(8,128)(2,1)S(1)}, bf16[128,2048]{1,0:T(8,128)(2,1)S(1)}, u32[]{:S(2)}, u32[]{:S(2)}) collective-permute-start(bf16[128,2048]{1,0:T(8,128)(2,1)S(1)} %copy-done.1), channel_id=1, source_target_pairs={{0,4},{2,6},{4,0},{6,2},{1,5},{3,7},{5,1},{7,3},{8,12},{10,14},{12... | collective-permute-start | bytes 1572872 | tf_op jit(solution)/shard_map/ppermute | solution.py:32
  114.9 2.2 %collective-permute-start.29 = (bf16[128,2048]{1,0:T(8,128)(2,1)S(1)}, bf16[128,2048]{1,0:T(8,128)(2,1)S(1)}, u32[]{:S(2)}, u32[]{:S(2)}) collective-permute-start(bf16[128,2048]{1,0:T(8,128)(2,1)S(1)} %get-tuple-element.58), channel_id=1, source_target_pairs={{0,6},{2,0},{4,2},{6,4},{1,7},{3,1},{5,3},{7,5},{8,14},{10,8},{12,... | collective-permute-start | bytes 1572872 | tf_op jit(solution)/shard_map/ppermute | solution.py:32
  118.6 4.9 %collective-permute-done.31.w2 = bf16[128,2048]{1,0:T(8,128)(2,1)S(1)} collective-permute-done((bf16[128,2048]{1,0:T(8,128)(2,1)S(1)}, bf16[128,2048]{1,0:T(8,128)(2,1)S(1)}, u32[]{:S(2)}, u32[]{:S(2)}) %collective-permute-start.31) | collective-permute-done | bytes 524320 | tf_op jit(solution)/shard_map/ppermute | solution.py:32
  125.4 9.5 %collective-permute-done.32.w3 = bf16[128,2048]{1,0:T(8,128)(2,1)S(1)} collective-permute-done((bf16[128,2048]{1,0:T(8,128)(2,1)S(1)}, bf16[128,2048]{1,0:T(8,128)(2,1)S(1)}, u32[]{:S(2)}, u32[]{:S(2)}) %collective-permute-start.32) | collective-permute-done | bytes 524320 | tf_op jit(solution)/shard_map/ppermute | solution.py:32
  134.9 2.4 %collective-permute-start.21 = (bf16[128,128]{1,0:T(8,128)(2,1)S(1)}, bf16[128,128]{1,0:T(8,128)(2,1)S(1)}, u32[]{:S(2)}, u32[]{:S(2)}) collective-permute-start(bf16[128,128]{1,0:T(8,128)(2,1)S(1)} %get-tuple-element.49), channel_id=1, source_target_pairs={{0,4},{2,6},{4,0},{6,2},{1,5},{3,7},{5,1},{7,3},{8,12},{10,14},{12... | collective-permute-start | bytes 98312 | tf_op jit(solution)/shard_map/ppermute | solution.py:32
  137.3 3.2 %collective-permute-done.27.g1 = bf16[128,2048]{1,0:T(8,128)(2,1)S(1)} collective-permute-done((bf16[128,2048]{1,0:T(8,128)(2,1)S(1)}, bf16[128,2048]{1,0:T(8,128)(2,1)S(1)}, u32[]{:S(2)}, u32[]{:S(2)}) %collective-permute-start.27) | collective-permute-done | bytes 524320 | tf_op jit(solution)/shard_map/ppermute | solution.py:32
  140.5 3.3 %collective-permute-done.28.g2 = bf16[128,2048]{1,0:T(8,128)(2,1)S(1)} collective-permute-done((bf16[128,2048]{1,0:T(8,128)(2,1)S(1)}, bf16[128,2048]{1,0:T(8,128)(2,1)S(1)}, u32[]{:S(2)}, u32[]{:S(2)}) %collective-permute-start.28) | collective-permute-done | bytes 524320 | tf_op jit(solution)/shard_map/ppermute | solution.py:32
  143.8 11.2 %collective-permute-done.29.g3 = bf16[128,2048]{1,0:T(8,128)(2,1)S(1)} collective-permute-done((bf16[128,2048]{1,0:T(8,128)(2,1)S(1)}, bf16[128,2048]{1,0:T(8,128)(2,1)S(1)}, u32[]{:S(2)}, u32[]{:S(2)}) %collective-permute-start.29) | collective-permute-done | bytes 524320 | tf_op jit(solution)/shard_map/ppermute | solution.py:32
  (71 shorter events, 44.0 us)
Async XLA Ops:
  1.8 9.4 %collective-permute-start = (bf16[64,2048]{1,0:T(8,128)(2,1)S(1)}, bf16[64,2048]{1,0:T(8,128)(2,1)S(1)}, u32[]{:S(2)}, u32[]{:S(2)}) collective-permute-start(bf16[64,2048]{1,0:T(8,128)(2,1)S(1)} %shard_map.131.n0), channel_id=1, source_target_pairs={{0,2},{2,4},{4,6},{6,0},{1,3},{3,5},{5,7},{7,1},{8,10},{10,12},{12... | collective-permute-start | bytes 786440 | tf_op jit(solution)/shard_map/ppermute | solution.py:32
  3.4 14.5 %collective-permute-start.1 = (bf16[64,2048]{1,0:T(8,128)(2,1)S(1)}, bf16[64,2048]{1,0:T(8,128)(2,1)S(1)}, u32[]{:S(2)}, u32[]{:S(2)}) collective-permute-start(bf16[64,2048]{1,0:T(8,128)(2,1)S(1)} %shard_map.131.n0), channel_id=1, source_target_pairs={{0,4},{2,6},{4,0},{6,2},{1,5},{3,7},{5,1},{7,3},{8,12},{10,14},{12... | collective-permute-start | bytes 786440 | tf_op jit(solution)/shard_map/ppermute | solution.py:32
  6.3 11.6 %collective-permute-start.2 = (bf16[64,2048]{1,0:T(8,128)(2,1)S(1)}, bf16[64,2048]{1,0:T(8,128)(2,1)S(1)}, u32[]{:S(2)}, u32[]{:S(2)}) collective-permute-start(bf16[64,2048]{1,0:T(8,128)(2,1)S(1)} %shard_map.131.n0), channel_id=1, source_target_pairs={{0,6},{2,0},{4,2},{6,4},{1,7},{3,1},{5,3},{7,5},{8,14},{10,8},{12,... | collective-permute-start | bytes 786440 | tf_op jit(solution)/shard_map/ppermute | solution.py:32
  7.7 14.9 %collective-permute-start.3 = (bf16[64,2048]{1,0:T(8,128)(2,1)S(1)}, bf16[64,2048]{1,0:T(8,128)(2,1)S(1)}, u32[]{:S(2)}, u32[]{:S(2)}) collective-permute-start(bf16[64,2048]{1,0:T(8,128)(2,1)S(1)} %shard_map.131.n0), channel_id=1, source_target_pairs={{0,1},{1,0},{2,3},{3,2},{4,5},{5,4},{6,7},{7,6},{8,9},{9,8},{10,11... | collective-permute-start | bytes 786440 | tf_op jit(solution)/shard_map/ppermute | solution.py:32
  11.2 11.4 %collective-permute-start.4 = (bf16[64,2048]{1,0:T(8,128)(2,1)S(1)}, bf16[64,2048]{1,0:T(8,128)(2,1)S(1)}, u32[]{:S(2)}, u32[]{:S(2)}) collective-permute-start(bf16[64,2048]{1,0:T(8,128)(2,1)S(1)} %collective-permute-done.n1), channel_id=1, source_target_pairs={{0,1},{1,0},{2,3},{3,2},{4,5},{5,4},{6,7},{7,6},{8,9},{9,8},{10,11... | collective-permute-start | bytes 786440 | tf_op jit(solution)/shard_map/ppermute | solution.py:32
  25.6 8.3 %collective-permute-start.10 = (bf16[1024,128]{1,0:T(8,128)(2,1)S(1)}, bf16[1024,128]{1,0:T(8,128)(2,1)S(1)}, u32[]{:S(2)}, u32[]{:S(2)}) collective-permute-start(bf16[1024,128]{1,0:T(8,128)(2,1)S(1)} %get-tuple-element.34.kv), channel_id=1, source_target_pairs={{0,32},{32,64},{64,96},{96,128},{128,160},{160,192},{192,224},{224... | collective-permute-start | bytes 786440 | tf_op jit(solution)/shard_map/ppermute | solution.py:32
  25.7 9.7 %collective-permute-start.14 = (bf16[1024,128]{1,0:T(8,128)(2,1)S(1)}, bf16[1024,128]{1,0:T(8,128)(2,1)S(1)}, u32[]{:S(2)}, u32[]{:S(2)}) collective-permute-start(bf16[1024,128]{1,0:T(8,128)(2,1)S(1)} %get-tuple-element.34.kv), channel_id=1, source_target_pairs={{0,224},{32,0},{64,32},{96,64},{128,96},{160,128},{192,160},{224,1... | collective-permute-start | bytes 786440 | tf_op jit(solution)/shard_map/ppermute | solution.py:32
  33.9 7.3 %collective-permute-start.11 = (bf16[1024,128]{1,0:T(8,128)(2,1)S(1)}, bf16[1024,128]{1,0:T(8,128)(2,1)S(1)}, u32[]{:S(2)}, u32[]{:S(2)}) collective-permute-start(bf16[1024,128]{1,0:T(8,128)(2,1)S(1)} %collective-permute-done.10.refs_3_), channel_id=1, source_target_pairs={{0,32},{32,64},{64,96},{96,128},{128,160},{160,192},{192,224},{224... | collective-permute-start | bytes 786440 | tf_op jit(solution)/shard_map/ppermute | solution.py:32
  35.4 11.1 %collective-permute-start.15 = (bf16[1024,128]{1,0:T(8,128)(2,1)S(1)}, bf16[1024,128]{1,0:T(8,128)(2,1)S(1)}, u32[]{:S(2)}, u32[]{:S(2)}) collective-permute-start(bf16[1024,128]{1,0:T(8,128)(2,1)S(1)} %collective-permute-done.14.refs_4_), channel_id=1, source_target_pairs={{0,224},{32,0},{64,32},{96,64},{128,96},{160,128},{192,160},{224,1... | collective-permute-start | bytes 786440 | tf_op jit(solution)/shard_map/ppermute | solution.py:32
  44.2 67.7 %collective-permute-start.30 = (bf16[128,2048]{1,0:T(8,128)(2,1)S(1)}, bf16[128,2048]{1,0:T(8,128)(2,1)S(1)}, u32[]{:S(2)}, u32[]{:S(2)}) collective-permute-start(bf16[128,2048]{1,0:T(8,128)(2,1)S(1)} %copy-done.1), channel_id=1, source_target_pairs={{0,2},{2,4},{4,6},{6,0},{1,3},{3,5},{5,7},{7,1},{8,10},{10,12},{12... | collective-permute-start | bytes 1572872 | tf_op jit(solution)/shard_map/ppermute | solution.py:32
  46.0 7.7 %collective-permute-start.7 = (bf16[128,512]{1,0:T(8,128)(2,1)S(1)}, bf16[128,512]{1,0:T(8,128)(2,1)S(1)}, u32[]{:S(2)}, u32[]{:S(2)}) collective-permute-start(bf16[128,512]{1,0:T(8,128)(2,1)S(1)} %get-tuple-element.33.q0), channel_id=1, source_target_pairs={{0,8},{8,16},{16,24},{24,0},{1,9},{9,17},{17,25},{25,1},{2,10},{10... | collective-permute-start | bytes 393224 | tf_op jit(solution)/shard_map/ppermute | solution.py:32
  46.5 27.9 %collective-permute-start.16 = (bf16[1024,128]{1,0:T(8,128)(2,1)S(1)}, bf16[1024,128]{1,0:T(8,128)(2,1)S(1)}, u32[]{:S(2)}, u32[]{:S(2)}) collective-permute-start(bf16[1024,128]{1,0:T(8,128)(2,1)S(1)} %collective-permute-done.15.refs_4_), channel_id=1, source_target_pairs={{0,224},{32,0},{64,32},{96,64},{128,96},{160,128},{192,160},{224,1... | collective-permute-start | bytes 786440 | tf_op jit(solution)/shard_map/ppermute | solution.py:32
  48.5 25.9 %collective-permute-start.13 = (bf16[1024,128]{1,0:T(8,128)(2,1)S(1)}, bf16[1024,128]{1,0:T(8,128)(2,1)S(1)}, u32[]{:S(2)}, u32[]{:S(2)}) collective-permute-start(bf16[1024,128]{1,0:T(8,128)(2,1)S(1)} %collective-permute-done.12.refs_3_), channel_id=1, source_target_pairs={{0,32},{32,64},{64,96},{96,128},{128,160},{160,192},{192,224},{224... | collective-permute-start | bytes 786440 | tf_op jit(solution)/shard_map/ppermute | solution.py:32
  83.4 29.9 %collective-permute-start.17 = (bf16[144,512]{1,0:T(8,128)(2,1)S(1)}, bf16[144,512]{1,0:T(8,128)(2,1)S(1)}, u32[]{:S(2)}, u32[]{:S(2)}) collective-permute-start(bf16[144,512]{1,0:T(8,128)(2,1)S(1)} %get-tuple-element.44), channel_id=1, source_target_pairs={{0,24},{8,0},{16,8},{24,16},{1,25},{9,1},{17,9},{25,17},{2,26},{10... | collective-permute-start | bytes 442376 | tf_op jit(solution)/shard_map/ppermute | solution.py:32
  84.2 29.8 %collective-permute-start.18 = (bf16[144,512]{1,0:T(8,128)(2,1)S(1)}, bf16[144,512]{1,0:T(8,128)(2,1)S(1)}, u32[]{:S(2)}, u32[]{:S(2)}) collective-permute-start(bf16[144,512]{1,0:T(8,128)(2,1)S(1)} %get-tuple-element.45), channel_id=1, source_target_pairs={{0,16},{8,24},{16,0},{24,8},{1,17},{9,25},{17,1},{25,9},{2,18},{10... | collective-permute-start | bytes 442376 | tf_op jit(solution)/shard_map/ppermute | solution.py:32
  87.8 27.1 %collective-permute-start.19 = (bf16[144,512]{1,0:T(8,128)(2,1)S(1)}, bf16[144,512]{1,0:T(8,128)(2,1)S(1)}, u32[]{:S(2)}, u32[]{:S(2)}) collective-permute-start(bf16[144,512]{1,0:T(8,128)(2,1)S(1)} %get-tuple-element.46), channel_id=1, source_target_pairs={{0,8},{8,16},{16,24},{24,0},{1,9},{9,17},{17,25},{25,1},{2,10},{10... | collective-permute-start | bytes 442376 | tf_op jit(solution)/shard_map/ppermute | solution.py:32
  107.1 16.3 %collective-permute-start.31 = (bf16[128,2048]{1,0:T(8,128)(2,1)S(1)}, bf16[128,2048]{1,0:T(8,128)(2,1)S(1)}, u32[]{:S(2)}, u32[]{:S(2)}) collective-permute-start(bf16[128,2048]{1,0:T(8,128)(2,1)S(1)} %copy-done.1), channel_id=1, source_target_pairs={{0,4},{2,6},{4,0},{6,2},{1,5},{3,7},{5,1},{7,3},{8,12},{10,14},{12... | collective-permute-start | bytes 1572872 | tf_op jit(solution)/shard_map/ppermute | solution.py:32
  111.9 23.0 %collective-permute-start.32 = (bf16[128,2048]{1,0:T(8,128)(2,1)S(1)}, bf16[128,2048]{1,0:T(8,128)(2,1)S(1)}, u32[]{:S(2)}, u32[]{:S(2)}) collective-permute-start(bf16[128,2048]{1,0:T(8,128)(2,1)S(1)} %copy-done.1), channel_id=1, source_target_pairs={{0,6},{2,0},{4,2},{6,4},{1,7},{3,1},{5,3},{7,5},{8,14},{10,8},{12,... | collective-permute-start | bytes 1572872 | tf_op jit(solution)/shard_map/ppermute | solution.py:32
  113.3 27.2 %collective-permute-start.27 = (bf16[128,2048]{1,0:T(8,128)(2,1)S(1)}, bf16[128,2048]{1,0:T(8,128)(2,1)S(1)}, u32[]{:S(2)}, u32[]{:S(2)}) collective-permute-start(bf16[128,2048]{1,0:T(8,128)(2,1)S(1)} %get-tuple-element.56), channel_id=1, source_target_pairs={{0,2},{2,4},{4,6},{6,0},{1,3},{3,5},{5,7},{7,1},{8,10},{10,12},{12... | collective-permute-start | bytes 1572872 | tf_op jit(solution)/shard_map/ppermute | solution.py:32
  114.0 29.8 %collective-permute-start.28 = (bf16[128,2048]{1,0:T(8,128)(2,1)S(1)}, bf16[128,2048]{1,0:T(8,128)(2,1)S(1)}, u32[]{:S(2)}, u32[]{:S(2)}) collective-permute-start(bf16[128,2048]{1,0:T(8,128)(2,1)S(1)} %get-tuple-element.57), channel_id=1, source_target_pairs={{0,4},{2,6},{4,0},{6,2},{1,5},{3,7},{5,1},{7,3},{8,12},{10,14},{12... | collective-permute-start | bytes 1572872 | tf_op jit(solution)/shard_map/ppermute | solution.py:32
  114.9 40.1 %collective-permute-start.29 = (bf16[128,2048]{1,0:T(8,128)(2,1)S(1)}, bf16[128,2048]{1,0:T(8,128)(2,1)S(1)}, u32[]{:S(2)}, u32[]{:S(2)}) collective-permute-start(bf16[128,2048]{1,0:T(8,128)(2,1)S(1)} %get-tuple-element.58), channel_id=1, source_target_pairs={{0,6},{2,0},{4,2},{6,4},{1,7},{3,1},{5,3},{7,5},{8,14},{10,8},{12,... | collective-permute-start | bytes 1572872 | tf_op jit(solution)/shard_map/ppermute | solution.py:32
  123.4 31.6 %collective-permute-start.20 = (bf16[128,128]{1,0:T(8,128)(2,1)S(1)}, bf16[128,128]{1,0:T(8,128)(2,1)S(1)}, u32[]{:S(2)}, u32[]{:S(2)}) collective-permute-start(bf16[128,128]{1,0:T(8,128)(2,1)S(1)} %get-tuple-element.48), channel_id=1, source_target_pairs={{0,2},{2,4},{4,6},{6,0},{1,3},{3,5},{5,7},{7,1},{8,10},{10,12},{12... | collective-permute-start | bytes 98312 | tf_op jit(solution)/shard_map/ppermute | solution.py:32
  134.9 20.1 %collective-permute-start.21 = (bf16[128,128]{1,0:T(8,128)(2,1)S(1)}, bf16[128,128]{1,0:T(8,128)(2,1)S(1)}, u32[]{:S(2)}, u32[]{:S(2)}) collective-permute-start(bf16[128,128]{1,0:T(8,128)(2,1)S(1)} %get-tuple-element.49), channel_id=1, source_target_pairs={{0,4},{2,6},{4,0},{6,2},{1,5},{3,7},{5,1},{7,3},{8,12},{10,14},{12... | collective-permute-start | bytes 98312 | tf_op jit(solution)/shard_map/ppermute | solution.py:32
  140.5 15.2 %collective-permute-start.22 = (bf16[128,128]{1,0:T(8,128)(2,1)S(1)}, bf16[128,128]{1,0:T(8,128)(2,1)S(1)}, u32[]{:S(2)}, u32[]{:S(2)}) collective-permute-start(bf16[128,128]{1,0:T(8,128)(2,1)S(1)} %get-tuple-element.50), channel_id=1, source_target_pairs={{0,6},{2,0},{4,2},{6,4},{1,7},{3,1},{5,3},{7,5},{8,14},{10,8},{12,... | collective-permute-start | bytes 98312 | tf_op jit(solution)/shard_map/ppermute | solution.py:32
  (15 other events, 161.8 us)

commit v2 on v1

--- a/solution.py
+++ b/solution.py
@@ -306,7 +306,7 @@
     z = place[2]
     count = 0
     for shift in shifts:
-        count = count + jnp.where(z >= shift % 8, 2, 0)
+        count = count + jnp.where(z >= shift % 8, 1, 0)
 
     def source(b):
         shift = jnp.int32(shifts[-1])
@@ -319,15 +319,12 @@
         for k, ref in enumerate(blocks):
             kvs[k] = ref[...]
 
-        def block(i):
-            return i // 2 if isinstance(i, int) else lax.shift_right_logical(i, 1)
-
         run_items(
-            2,
+            4,
             count,
-            block,
-            lambda i: source(block(i)),
-            lambda i: 2 * (i % 2) if isinstance(i, int) else 2 * lax.bitwise_and(i, 1),
+            lambda i: i,
+            source,
+            lambda i: 0,
             None,
             q, kvs, bias, acc, best, s_buf, top, p_buf, shrink,
         )

time: 161 us -> 161 us (level)
  transfers between devices with their start and end apart: 34 -> 34, of which waited for: 18 -> 18; matrix products, arithmetic and copies ran while one was open for 0% -> 0% of each run, Pallas kernels for 20% -> 19%
where the time goes in v2:
time: 161 us; the launch traced here: 159 us
  waiting for transfers between devices  73.4 us (46%)
  starting transfers between devices  46.5 us (29%)
  Pallas kernels  36.7 us (23%)
    ppermute x31, waiting for transfers between devices, turn(): return lax.ppermute(array, axis, [(i, (i + by) % n) for i in range(n)])  65.8 us
    ppermute x31, starting transfers between devices, turn(): return lax.ppermute(array, axis, [(i, (i + by) % n) for i in range(n)])  39.7 us
    pallas_call x13, Pallas kernels, kernel(): pl.pallas_call(body, out_shape=outs, in_specs=specs + [pl.BlockSpec(memor...  36.7 us
    ppermute x2, starting transfers between devices, swap(): return lax.ppermute(array, axis, [(i, i ^ bit) for i in range(n)])  5.56 us
    ppermute x1, waiting for transfers between devices, per_device(): rim = lax.ppermute(rim, ('z', 'x'), [(i, i + 1) for i in range(31)])  4.33 us
    ppermute x2, waiting for transfers between devices, swap(): return lax.ppermute(array, axis, [(i, i ^ bit) for i in range(n)])  3.31 us
  transfers between devices with their start and end apart: 34, of which 18 were waited for; matrix products, arithmetic and copies ran while one was open for 0% of the time, Pallas kernels for 19%

profile of v2, /device:TPU:230, one launch (start us, length us, event | category | flops | bytes accessed | tf_op | source)
XLA Modules:
  0.0 158.6 jit_solution(6208418912900818949)
XLA Ops:
  3.4 2.9 %collective-permute-start.1 = (bf16[64,2048]{1,0:T(8,128)(2,1)S(1)}, bf16[64,2048]{1,0:T(8,128)(2,1)S(1)}, u32[]{:S(2)}, u32[]{:S(2)}) collective-permute-start(bf16[64,2048]{1,0:T(8,128)(2,1)S(1)} %shard_map.131.n0), channel_id=1, source_target_pairs={{0,4},{2,6},{4,0},{6,2},{1,5},{3,7},{5,1},{7,3},{8,12},{10,14},{12... | collective-permute-start | bytes 786440 | tf_op jit(solution)/shard_map/ppermute | solution.py:32
  7.7 3.5 %collective-permute-done.n1 = bf16[64,2048]{1,0:T(8,128)(2,1)S(1)} collective-permute-done((bf16[64,2048]{1,0:T(8,128)(2,1)S(1)}, bf16[64,2048]{1,0:T(8,128)(2,1)S(1)}, u32[]{:S(2)}, u32[]{:S(2)}) %collective-permute-start) | collective-permute-done | bytes 262176 | tf_op jit(solution)/shard_map/ppermute | solution.py:32
  11.2 6.8 %collective-permute-done.1.n2 = bf16[64,2048]{1,0:T(8,128)(2,1)S(1)} collective-permute-done((bf16[64,2048]{1,0:T(8,128)(2,1)S(1)}, bf16[64,2048]{1,0:T(8,128)(2,1)S(1)}, u32[]{:S(2)}, u32[]{:S(2)}) %collective-permute-start.1) | collective-permute-done | bytes 262176 | tf_op jit(solution)/shard_map/ppermute | solution.py:32
  22.6 3.0 %shard_map.134 = (bf16[128,512]{1,0:T(8,128)(2,1)S(1)}, bf16[1024,128]{1,0:T(8,128)(2,1)S(1)}, bf16[512,256]{1,0:T(8,128)(2,1)S(1)}, bf16[32,256]{1,0:T(8,128)(2,1)S(1)}) custom-call(s32[4]{0:T(128)S(1)} %pad_add_fusion.place.refs_0_, bf16[64,2048]{1,0:T(8,128)(2,1)S(1)} %shard_map.131.n0, bf16[64,2048]{1,0:T(8,128)(2,1)S(1)} %collective-permute-done.n1, ...), custom_call_target="tpu_custom_call" | custom-call | tf_op jit(solution)/shard_map/pallas_call | solution.py:45
  27.7 6.2 %collective-permute-done.10.refs_3_ = bf16[1024,128]{1,0:T(8,128)(2,1)S(1)} collective-permute-done((bf16[1024,128]{1,0:T(8,128)(2,1)S(1)}, bf16[1024,128]{1,0:T(8,128)(2,1)S(1)}, u32[]{:S(2)}, u32[]{:S(2)}) %collective-permute-start.10) | collective-permute-done | bytes 262176 | tf_op jit(solution)/shard_map/ppermute | solution.py:32
  35.9 5.3 %collective-permute-done.11.refs_3_ = bf16[1024,128]{1,0:T(8,128)(2,1)S(1)} collective-permute-done((bf16[1024,128]{1,0:T(8,128)(2,1)S(1)}, bf16[1024,128]{1,0:T(8,128)(2,1)S(1)}, u32[]{:S(2)}, u32[]{:S(2)}) %collective-permute-start.11) | collective-permute-done | bytes 262176 | tf_op jit(solution)/shard_map/ppermute | solution.py:32
  41.2 3.0 %collective-permute-start.12 = (bf16[1024,128]{1,0:T(8,128)(2,1)S(1)}, bf16[1024,128]{1,0:T(8,128)(2,1)S(1)}, u32[]{:S(2)}, u32[]{:S(2)}) collective-permute-start(bf16[1024,128]{1,0:T(8,128)(2,1)S(1)} %collective-permute-done.11.refs_3_), channel_id=1, source_target_pairs={{0,32},{32,64},{64,96},{96,128},{128,160},{160,192},{192,224},{224... | collective-permute-start | bytes 786440 | tf_op jit(solution)/shard_map/ppermute | solution.py:32
  48.5 3.7 %collective-permute-start.13 = (bf16[1024,128]{1,0:T(8,128)(2,1)S(1)}, bf16[1024,128]{1,0:T(8,128)(2,1)S(1)}, u32[]{:S(2)}, u32[]{:S(2)}) collective-permute-start(bf16[1024,128]{1,0:T(8,128)(2,1)S(1)} %collective-permute-done.12.refs_3_), channel_id=1, source_target_pairs={{0,32},{32,64},{64,96},{96,128},{128,160},{160,192},{192,224},{224... | collective-permute-start | bytes 786440 | tf_op jit(solution)/shard_map/ppermute | solution.py:32
  53.6 5.1 %collective-permute-done.8.q2 = bf16[128,512]{1,0:T(8,128)(2,1)S(1)} collective-permute-done((bf16[128,512]{1,0:T(8,128)(2,1)S(1)}, bf16[128,512]{1,0:T(8,128)(2,1)S(1)}, u32[]{:S(2)}, u32[]{:S(2)}) %collective-permute-start.8) | collective-permute-done | bytes 131104 | tf_op jit(solution)/shard_map/ppermute | solution.py:32
  62.0 6.0 %shard_map.136 = (f32[4,2,80,512]{3,2,1,0:T(8,128)S(1)}, f32[4,2,1,512]{3,2,1,0:T(1,128)S(1)}) custom-call(s32[4]{0:T(128)S(1)} %pad_add_fusion.place.refs_0_, bf16[4,128,512]{2,1,0:T(8,128)(2,1)S(1)} %get-tuple-element.36.refs_1_, bf16[8,512,128]{2,1,0:T(8,128)(2,1)S(1)} %get-tuple-element.35.bias.refs_2_, ...), custom_call_target="tpu_custom_call", output_to_operand_aliasing={{0}: (5, {}), {1}: (6, {})} | custom-call | tf_op jit(solution)/shard_map/pallas_call | solution.py:45
  67.9 6.0 %shard_map.137 = (f32[4,2,80,512]{3,2,1,0:T(8,128)S(1)}, f32[4,2,1,512]{3,2,1,0:T(1,128)S(1)}) custom-call(s32[4]{0:T(128)S(1)} %pad_add_fusion.place.refs_0_, bf16[4,128,512]{2,1,0:T(8,128)(2,1)S(1)} %get-tuple-element.36.refs_1_, bf16[8,512,128]{2,1,0:T(8,128)(2,1)S(1)} %get-tuple-element.35.bias.refs_2_, ...), custom_call_target="tpu_custom_call", output_to_operand_aliasing={{0}: (5, {}), {1}: (6, {})} | custom-call | tf_op jit(solution)/shard_map/pallas_call | solution.py:45
  74.0 8.7 %shard_map.138 = (bf16[144,512]{1,0:T(8,128)(2,1)S(1)}, bf16[144,512]{1,0:T(8,128)(2,1)S(1)}, bf16[144,512]{1,0:T(8,128)(2,1)S(1)}, bf16[144,512]{1,0:T(8,128)(2...) custom-call(s32[4]{0:T(128)S(1)} %pad_add_fusion.place.refs_0_, ...), custom_call_target="tpu_custom_call", output_to_operand_aliasing={{4}: (6, {}), {5}: (7, {})} | custom-call | tf_op jit(solution)/shard_map/pallas_call | solution.py:45
  83.5 3.7 %collective-permute-start.18 = (bf16[144,512]{1,0:T(8,128)(2,1)S(1)}, bf16[144,512]{1,0:T(8,128)(2,1)S(1)}, u32[]{:S(2)}, u32[]{:S(2)}) collective-permute-start(bf16[144,512]{1,0:T(8,128)(2,1)S(1)} %get-tuple-element.45), channel_id=1, source_target_pairs={{0,16},{8,24},{16,0},{24,8},{1,17},{9,25},{17,1},{25,9},{2,18},{10... | collective-permute-start | bytes 442376 | tf_op jit(solution)/shard_map/ppermute | solution.py:32
  89.6 4.3 %collective-permute-done.23.rim = bf16[32,256]{1,0:T(8,128)(2,1)S(1)} collective-permute-done((bf16[32,256]{1,0:T(8,128)(2,1)S(1)}, bf16[32,256]{1,0:T(8,128)(2,1)S(1)}, u32[]{:S(2)}, u32[]{:S(2)}) %collective-permute-start.23) | collective-permute-done | bytes 16416 | tf_op jit(solution)/shard_map/ppermute | solution.py:447
  94.0 2.2 %shard_map.140 = (f32[512,256]{1,0:T(8,128)S(1)}, f32[1,512]{1,0:T(1,128)S(1)}) custom-call(bf16[512,256]{1,0:T(8,128)(2,1)S(1)} %get-tuple-element.51.gated, bf16[32,256]{1,0:T(8,128)(2,1)S(1)} %collective-permute-done.23.rim, f32[31,256]{1,0:T(8,128)S(1)} %copy-done.3), custom_call_target="tpu_custom_call" | custom-call | tf_op jit(solution)/shard_map/pallas_call | solution.py:45
  101.3 3.3 %collective-permute-start.26 = (f32[1,512]{1,0:T(1,128)S(1)}, f32[1,512]{1,0:T(1,128)S(1)}, u32[]{:S(2)}, u32[]{:S(2)}) collective-permute-start(f32[1,512]{1,0:T(1,128)S(1)} %add.10), channel_id=1, source_target_pairs={{0,4},{2,6},{4,0},{6,2},{1,5},{3,7},{5,1},{7,3},{8,12},{10,14},{12... | collective-permute-start | bytes 6152 | tf_op jit(solution)/shard_map/ppermute | solution.py:37
  106.4 3.3 %collective-permute-start.31 = (bf16[128,2048]{1,0:T(8,128)(2,1)S(1)}, bf16[128,2048]{1,0:T(8,128)(2,1)S(1)}, u32[]{:S(2)}, u32[]{:S(2)}) collective-permute-start(bf16[128,2048]{1,0:T(8,128)(2,1)S(1)} %copy-done.1), channel_id=1, source_target_pairs={{0,4},{2,6},{4,0},{6,2},{1,5},{3,7},{5,1},{7,3},{8,12},{10,14},{12... | collective-permute-start | bytes 1572872 | tf_op jit(solution)/shard_map/ppermute | solution.py:32
  114.2 2.2 %collective-permute-start.29 = (bf16[128,2048]{1,0:T(8,128)(2,1)S(1)}, bf16[128,2048]{1,0:T(8,128)(2,1)S(1)}, u32[]{:S(2)}, u32[]{:S(2)}) collective-permute-start(bf16[128,2048]{1,0:T(8,128)(2,1)S(1)} %get-tuple-element.58), channel_id=1, source_target_pairs={{0,6},{2,0},{4,2},{6,4},{1,7},{3,1},{5,3},{7,5},{8,14},{10,8},{12,... | collective-permute-start | bytes 1572872 | tf_op jit(solution)/shard_map/ppermute | solution.py:32
  117.8 4.9 %collective-permute-done.31.w2 = bf16[128,2048]{1,0:T(8,128)(2,1)S(1)} collective-permute-done((bf16[128,2048]{1,0:T(8,128)(2,1)S(1)}, bf16[128,2048]{1,0:T(8,128)(2,1)S(1)}, u32[]{:S(2)}, u32[]{:S(2)}) %collective-permute-start.31) | collective-permute-done | bytes 524320 | tf_op jit(solution)/shard_map/ppermute | solution.py:32
  124.7 9.5 %collective-permute-done.32.w3 = bf16[128,2048]{1,0:T(8,128)(2,1)S(1)} collective-permute-done((bf16[128,2048]{1,0:T(8,128)(2,1)S(1)}, bf16[128,2048]{1,0:T(8,128)(2,1)S(1)}, u32[]{:S(2)}, u32[]{:S(2)}) %collective-permute-start.32) | collective-permute-done | bytes 524320 | tf_op jit(solution)/shard_map/ppermute | solution.py:32
  134.2 2.4 %collective-permute-start.21 = (bf16[128,128]{1,0:T(8,128)(2,1)S(1)}, bf16[128,128]{1,0:T(8,128)(2,1)S(1)}, u32[]{:S(2)}, u32[]{:S(2)}) collective-permute-start(bf16[128,128]{1,0:T(8,128)(2,1)S(1)} %get-tuple-element.49), channel_id=1, source_target_pairs={{0,4},{2,6},{4,0},{6,2},{1,5},{3,7},{5,1},{7,3},{8,12},{10,14},{12... | collective-permute-start | bytes 98312 | tf_op jit(solution)/shard_map/ppermute | solution.py:32
  136.6 3.2 %collective-permute-done.27.g1 = bf16[128,2048]{1,0:T(8,128)(2,1)S(1)} collective-permute-done((bf16[128,2048]{1,0:T(8,128)(2,1)S(1)}, bf16[128,2048]{1,0:T(8,128)(2,1)S(1)}, u32[]{:S(2)}, u32[]{:S(2)}) %collective-permute-start.27) | collective-permute-done | bytes 524320 | tf_op jit(solution)/shard_map/ppermute | solution.py:32
  139.8 3.3 %collective-permute-done.28.g2 = bf16[128,2048]{1,0:T(8,128)(2,1)S(1)} collective-permute-done((bf16[128,2048]{1,0:T(8,128)(2,1)S(1)}, bf16[128,2048]{1,0:T(8,128)(2,1)S(1)}, u32[]{:S(2)}, u32[]{:S(2)}) %collective-permute-start.28) | collective-permute-done | bytes 524320 | tf_op jit(solution)/shard_map/ppermute | solution.py:32
  143.1 11.2 %collective-permute-done.29.g3 = bf16[128,2048]{1,0:T(8,128)(2,1)S(1)} collective-permute-done((bf16[128,2048]{1,0:T(8,128)(2,1)S(1)}, bf16[128,2048]{1,0:T(8,128)(2,1)S(1)}, u32[]{:S(2)}, u32[]{:S(2)}) %collective-permute-start.29) | collective-permute-done | bytes 524320 | tf_op jit(solution)/shard_map/ppermute | solution.py:32
  (71 shorter events, 44.0 us)
Async XLA Ops:
  1.8 9.4 %collective-permute-start = (bf16[64,2048]{1,0:T(8,128)(2,1)S(1)}, bf16[64,2048]{1,0:T(8,128)(2,1)S(1)}, u32[]{:S(2)}, u32[]{:S(2)}) collective-permute-start(bf16[64,2048]{1,0:T(8,128)(2,1)S(1)} %shard_map.131.n0), channel_id=1, source_target_pairs={{0,2},{2,4},{4,6},{6,0},{1,3},{3,5},{5,7},{7,1},{8,10},{10,12},{12... | collective-permute-start | bytes 786440 | tf_op jit(solution)/shard_map/ppermute | solution.py:32
  3.4 14.5 %collective-permute-start.1 = (bf16[64,2048]{1,0:T(8,128)(2,1)S(1)}, bf16[64,2048]{1,0:T(8,128)(2,1)S(1)}, u32[]{:S(2)}, u32[]{:S(2)}) collective-permute-start(bf16[64,2048]{1,0:T(8,128)(2,1)S(1)} %shard_map.131.n0), channel_id=1, source_target_pairs={{0,4},{2,6},{4,0},{6,2},{1,5},{3,7},{5,1},{7,3},{8,12},{10,14},{12... | collective-permute-start | bytes 786440 | tf_op jit(solution)/shard_map/ppermute | solution.py:32
  6.3 11.6 %collective-permute-start.2 = (bf16[64,2048]{1,0:T(8,128)(2,1)S(1)}, bf16[64,2048]{1,0:T(8,128)(2,1)S(1)}, u32[]{:S(2)}, u32[]{:S(2)}) collective-permute-start(bf16[64,2048]{1,0:T(8,128)(2,1)S(1)} %shard_map.131.n0), channel_id=1, source_target_pairs={{0,6},{2,0},{4,2},{6,4},{1,7},{3,1},{5,3},{7,5},{8,14},{10,8},{12,... | collective-permute-start | bytes 786440 | tf_op jit(solution)/shard_map/ppermute | solution.py:32
  7.7 14.9 %collective-permute-start.3 = (bf16[64,2048]{1,0:T(8,128)(2,1)S(1)}, bf16[64,2048]{1,0:T(8,128)(2,1)S(1)}, u32[]{:S(2)}, u32[]{:S(2)}) collective-permute-start(bf16[64,2048]{1,0:T(8,128)(2,1)S(1)} %shard_map.131.n0), channel_id=1, source_target_pairs={{0,1},{1,0},{2,3},{3,2},{4,5},{5,4},{6,7},{7,6},{8,9},{9,8},{10,11... | collective-permute-start | bytes 786440 | tf_op jit(solution)/shard_map/ppermute | solution.py:32
  11.2 11.4 %collective-permute-start.4 = (bf16[64,2048]{1,0:T(8,128)(2,1)S(1)}, bf16[64,2048]{1,0:T(8,128)(2,1)S(1)}, u32[]{:S(2)}, u32[]{:S(2)}) collective-permute-start(bf16[64,2048]{1,0:T(8,128)(2,1)S(1)} %collective-permute-done.n1), channel_id=1, source_target_pairs={{0,1},{1,0},{2,3},{3,2},{4,5},{5,4},{6,7},{7,6},{8,9},{9,8},{10,11... | collective-permute-start | bytes 786440 | tf_op jit(solution)/shard_map/ppermute | solution.py:32
  25.6 8.3 %collective-permute-start.10 = (bf16[1024,128]{1,0:T(8,128)(2,1)S(1)}, bf16[1024,128]{1,0:T(8,128)(2,1)S(1)}, u32[]{:S(2)}, u32[]{:S(2)}) collective-permute-start(bf16[1024,128]{1,0:T(8,128)(2,1)S(1)} %get-tuple-element.34.kv), channel_id=1, source_target_pairs={{0,32},{32,64},{64,96},{96,128},{128,160},{160,192},{192,224},{224... | collective-permute-start | bytes 786440 | tf_op jit(solution)/shard_map/ppermute | solution.py:32
  25.7 9.7 %collective-permute-start.14 = (bf16[1024,128]{1,0:T(8,128)(2,1)S(1)}, bf16[1024,128]{1,0:T(8,128)(2,1)S(1)}, u32[]{:S(2)}, u32[]{:S(2)}) collective-permute-start(bf16[1024,128]{1,0:T(8,128)(2,1)S(1)} %get-tuple-element.34.kv), channel_id=1, source_target_pairs={{0,224},{32,0},{64,32},{96,64},{128,96},{160,128},{192,160},{224,1... | collective-permute-start | bytes 786440 | tf_op jit(solution)/shard_map/ppermute | solution.py:32
  33.9 7.3 %collective-permute-start.11 = (bf16[1024,128]{1,0:T(8,128)(2,1)S(1)}, bf16[1024,128]{1,0:T(8,128)(2,1)S(1)}, u32[]{:S(2)}, u32[]{:S(2)}) collective-permute-start(bf16[1024,128]{1,0:T(8,128)(2,1)S(1)} %collective-permute-done.10.refs_3_), channel_id=1, source_target_pairs={{0,32},{32,64},{64,96},{96,128},{128,160},{160,192},{192,224},{224... | collective-permute-start | bytes 786440 | tf_op jit(solution)/shard_map/ppermute | solution.py:32
  35.4 11.1 %collective-permute-start.15 = (bf16[1024,128]{1,0:T(8,128)(2,1)S(1)}, bf16[1024,128]{1,0:T(8,128)(2,1)S(1)}, u32[]{:S(2)}, u32[]{:S(2)}) collective-permute-start(bf16[1024,128]{1,0:T(8,128)(2,1)S(1)} %collective-permute-done.14.refs_4_), channel_id=1, source_target_pairs={{0,224},{32,0},{64,32},{96,64},{128,96},{160,128},{192,160},{224,1... | collective-permute-start | bytes 786440 | tf_op jit(solution)/shard_map/ppermute | solution.py:32
  44.2 66.9 %collective-permute-start.30 = (bf16[128,2048]{1,0:T(8,128)(2,1)S(1)}, bf16[128,2048]{1,0:T(8,128)(2,1)S(1)}, u32[]{:S(2)}, u32[]{:S(2)}) collective-permute-start(bf16[128,2048]{1,0:T(8,128)(2,1)S(1)} %copy-done.1), channel_id=1, source_target_pairs={{0,2},{2,4},{4,6},{6,0},{1,3},{3,5},{5,7},{7,1},{8,10},{10,12},{12... | collective-permute-start | bytes 1572872 | tf_op jit(solution)/shard_map/ppermute | solution.py:32
  46.0 7.7 %collective-permute-start.7 = (bf16[128,512]{1,0:T(8,128)(2,1)S(1)}, bf16[128,512]{1,0:T(8,128)(2,1)S(1)}, u32[]{:S(2)}, u32[]{:S(2)}) collective-permute-start(bf16[128,512]{1,0:T(8,128)(2,1)S(1)} %get-tuple-element.33.q0), channel_id=1, source_target_pairs={{0,8},{8,16},{16,24},{24,0},{1,9},{9,17},{17,25},{25,1},{2,10},{10... | collective-permute-start | bytes 393224 | tf_op jit(solution)/shard_map/ppermute | solution.py:32
  46.5 27.5 %collective-permute-start.16 = (bf16[1024,128]{1,0:T(8,128)(2,1)S(1)}, bf16[1024,128]{1,0:T(8,128)(2,1)S(1)}, u32[]{:S(2)}, u32[]{:S(2)}) collective-permute-start(bf16[1024,128]{1,0:T(8,128)(2,1)S(1)} %collective-permute-done.15.refs_4_), channel_id=1, source_target_pairs={{0,224},{32,0},{64,32},{96,64},{128,96},{160,128},{192,160},{224,1... | collective-permute-start | bytes 786440 | tf_op jit(solution)/shard_map/ppermute | solution.py:32
  48.5 25.4 %collective-permute-start.13 = (bf16[1024,128]{1,0:T(8,128)(2,1)S(1)}, bf16[1024,128]{1,0:T(8,128)(2,1)S(1)}, u32[]{:S(2)}, u32[]{:S(2)}) collective-permute-start(bf16[1024,128]{1,0:T(8,128)(2,1)S(1)} %collective-permute-done.12.refs_3_), channel_id=1, source_target_pairs={{0,32},{32,64},{64,96},{96,128},{128,160},{160,192},{192,224},{224... | collective-permute-start | bytes 786440 | tf_op jit(solution)/shard_map/ppermute | solution.py:32
  82.7 29.9 %collective-permute-start.17 = (bf16[144,512]{1,0:T(8,128)(2,1)S(1)}, bf16[144,512]{1,0:T(8,128)(2,1)S(1)}, u32[]{:S(2)}, u32[]{:S(2)}) collective-permute-start(bf16[144,512]{1,0:T(8,128)(2,1)S(1)} %get-tuple-element.44), channel_id=1, source_target_pairs={{0,24},{8,0},{16,8},{24,16},{1,25},{9,1},{17,9},{25,17},{2,26},{10... | collective-permute-start | bytes 442376 | tf_op jit(solution)/shard_map/ppermute | solution.py:32
  83.5 29.8 %collective-permute-start.18 = (bf16[144,512]{1,0:T(8,128)(2,1)S(1)}, bf16[144,512]{1,0:T(8,128)(2,1)S(1)}, u32[]{:S(2)}, u32[]{:S(2)}) collective-permute-start(bf16[144,512]{1,0:T(8,128)(2,1)S(1)} %get-tuple-element.45), channel_id=1, source_target_pairs={{0,16},{8,24},{16,0},{24,8},{1,17},{9,25},{17,1},{25,9},{2,18},{10... | collective-permute-start | bytes 442376 | tf_op jit(solution)/shard_map/ppermute | solution.py:32
  87.1 27.1 %collective-permute-start.19 = (bf16[144,512]{1,0:T(8,128)(2,1)S(1)}, bf16[144,512]{1,0:T(8,128)(2,1)S(1)}, u32[]{:S(2)}, u32[]{:S(2)}) collective-permute-start(bf16[144,512]{1,0:T(8,128)(2,1)S(1)} %get-tuple-element.46), channel_id=1, source_target_pairs={{0,8},{8,16},{16,24},{24,0},{1,9},{9,17},{17,25},{25,1},{2,10},{10... | collective-permute-start | bytes 442376 | tf_op jit(solution)/shard_map/ppermute | solution.py:32
  106.4 16.3 %collective-permute-start.31 = (bf16[128,2048]{1,0:T(8,128)(2,1)S(1)}, bf16[128,2048]{1,0:T(8,128)(2,1)S(1)}, u32[]{:S(2)}, u32[]{:S(2)}) collective-permute-start(bf16[128,2048]{1,0:T(8,128)(2,1)S(1)} %copy-done.1), channel_id=1, source_target_pairs={{0,4},{2,6},{4,0},{6,2},{1,5},{3,7},{5,1},{7,3},{8,12},{10,14},{12... | collective-permute-start | bytes 1572872 | tf_op jit(solution)/shard_map/ppermute | solution.py:32
  111.2 23.0 %collective-permute-start.32 = (bf16[128,2048]{1,0:T(8,128)(2,1)S(1)}, bf16[128,2048]{1,0:T(8,128)(2,1)S(1)}, u32[]{:S(2)}, u32[]{:S(2)}) collective-permute-start(bf16[128,2048]{1,0:T(8,128)(2,1)S(1)} %copy-done.1), channel_id=1, source_target_pairs={{0,6},{2,0},{4,2},{6,4},{1,7},{3,1},{5,3},{7,5},{8,14},{10,8},{12,... | collective-permute-start | bytes 1572872 | tf_op jit(solution)/shard_map/ppermute | solution.py:32
  112.6 27.2 %collective-permute-start.27 = (bf16[128,2048]{1,0:T(8,128)(2,1)S(1)}, bf16[128,2048]{1,0:T(8,128)(2,1)S(1)}, u32[]{:S(2)}, u32[]{:S(2)}) collective-permute-start(bf16[128,2048]{1,0:T(8,128)(2,1)S(1)} %get-tuple-element.56), channel_id=1, source_target_pairs={{0,2},{2,4},{4,6},{6,0},{1,3},{3,5},{5,7},{7,1},{8,10},{10,12},{12... | collective-permute-start | bytes 1572872 | tf_op jit(solution)/shard_map/ppermute | solution.py:32
  113.3 29.8 %collective-permute-start.28 = (bf16[128,2048]{1,0:T(8,128)(2,1)S(1)}, bf16[128,2048]{1,0:T(8,128)(2,1)S(1)}, u32[]{:S(2)}, u32[]{:S(2)}) collective-permute-start(bf16[128,2048]{1,0:T(8,128)(2,1)S(1)} %get-tuple-element.57), channel_id=1, source_target_pairs={{0,4},{2,6},{4,0},{6,2},{1,5},{3,7},{5,1},{7,3},{8,12},{10,14},{12... | collective-permute-start | bytes 1572872 | tf_op jit(solution)/shard_map/ppermute | solution.py:32
  114.2 40.1 %collective-permute-start.29 = (bf16[128,2048]{1,0:T(8,128)(2,1)S(1)}, bf16[128,2048]{1,0:T(8,128)(2,1)S(1)}, u32[]{:S(2)}, u32[]{:S(2)}) collective-permute-start(bf16[128,2048]{1,0:T(8,128)(2,1)S(1)} %get-tuple-element.58), channel_id=1, source_target_pairs={{0,6},{2,0},{4,2},{6,4},{1,7},{3,1},{5,3},{7,5},{8,14},{10,8},{12,... | collective-permute-start | bytes 1572872 | tf_op jit(solution)/shard_map/ppermute | solution.py:32
  122.7 31.6 %collective-permute-start.20 = (bf16[128,128]{1,0:T(8,128)(2,1)S(1)}, bf16[128,128]{1,0:T(8,128)(2,1)S(1)}, u32[]{:S(2)}, u32[]{:S(2)}) collective-permute-start(bf16[128,128]{1,0:T(8,128)(2,1)S(1)} %get-tuple-element.48), channel_id=1, source_target_pairs={{0,2},{2,4},{4,6},{6,0},{1,3},{3,5},{5,7},{7,1},{8,10},{10,12},{12... | collective-permute-start | bytes 98312 | tf_op jit(solution)/shard_map/ppermute | solution.py:32
  134.2 20.1 %collective-permute-start.21 = (bf16[128,128]{1,0:T(8,128)(2,1)S(1)}, bf16[128,128]{1,0:T(8,128)(2,1)S(1)}, u32[]{:S(2)}, u32[]{:S(2)}) collective-permute-start(bf16[128,128]{1,0:T(8,128)(2,1)S(1)} %get-tuple-element.49), channel_id=1, source_target_pairs={{0,4},{2,6},{4,0},{6,2},{1,5},{3,7},{5,1},{7,3},{8,12},{10,14},{12... | collective-permute-start | bytes 98312 | tf_op jit(solution)/shard_map/ppermute | solution.py:32
  139.8 15.2 %collective-permute-start.22 = (bf16[128,128]{1,0:T(8,128)(2,1)S(1)}, bf16[128,128]{1,0:T(8,128)(2,1)S(1)}, u32[]{:S(2)}, u32[]{:S(2)}) collective-permute-start(bf16[128,128]{1,0:T(8,128)(2,1)S(1)} %get-tuple-element.50), channel_id=1, source_target_pairs={{0,6},{2,0},{4,2},{6,4},{1,7},{3,1},{5,3},{7,5},{8,14},{10,8},{12,... | collective-permute-start | bytes 98312 | tf_op jit(solution)/shard_map/ppermute | solution.py:32
  (15 other events, 160.9 us)
